TPU v7x, 32 devices: a whole 2x2x4 slice. The times are simulated.
32 devices in a mesh: ep: 8 (over z, y), tp: 4 (over x, core).
Axes of the slice: x: 2, y: 2, z: 4, core: 2. Of those that a mesh axis runs over, the one named last changes fastest.
Arguments:
- queries: bfloat16 [1536, 8, 128], P('ep', 'tp'), may hold values from -140 to 140
- keys: bfloat16 [1536, 4, 128], P('ep', 'tp'), may hold values from -6 to 6
- values: bfloat16 [1536, 4, 128], P('ep', 'tp'), may hold values from -6 to 6
- mix_scale: float32 [8], P('tp'), may hold values from 0.3 to 0.8
- head_gain: float32 [128], replicated, may hold values from 0.1 to 1.9
- out_weight: bfloat16 [8, 128, 2048], P('tp'), may hold values from -0.1875 to 0.1875
- moe_input: bfloat16 [3072, 2048], P(('ep', 'tp')), may hold values from -6 to 6
- norm_gain: float32 [2048], replicated, may hold values from 0.1 to 1.9
- routes: int32 [3072, 2], P(('ep', 'tp')), may hold values from 0 to 7, all different within a row; in each aligned block of 96 rows (0 to 95, 96 to 191, ...) at most 36 rows name the same one
- route_weights: float32 [3072, 2], P(('ep', 'tp')), may hold values from 0.2 to 1
- gate_weight: bfloat16 [8, 2048, 3584], P('ep', None, 'tp'), may hold values from -0.125 to 0.125
- up_weight: bfloat16 [8, 2048, 3584], P('ep', None, 'tp'), may hold values from -0.125 to 0.125
- down_weight: bfloat16 [8, 3584, 2048], P('ep', 'tp'), may hold values from -0.09375 to 0.09375
Outputs:
- attn_out: bfloat16 [1536, 2048], P(('ep', 'tp'))
- moe_out: bfloat16 [3072, 2048], P(('ep', 'tp'))
Inputs may be any that keep to these rules, and one draw needn't show every extreme that they name: `routes`: the 2 experts of a row differ. In each aligned block of 96 rows (the rows of one device) no expert is named by more than 36 rows, and in some blocks an expert is named by exactly 36 rows.
All inputs are finite; a program needn't handle non-finite values.
Results may differ from a plain program's by a relative error of at most 0.014.
Values may be sent and summed in bfloat16 or wider, within the bound.
No kernel may reach another device: no remote copies, remote signals or barrier semaphores. Data moves between devices by JAX's collectives and lax.ppermute only.
A program may use at most 128 MiB of HBM per device.

v0:
```python
import functools
import math

import jax
import jax.numpy as jnp
from jax import lax
from jax.experimental import pallas as pl
from jax.experimental.pallas import tpu as pltpu
from jax.sharding import PartitionSpec as P

NEG_LARGE = -1e30
VMEM_LIMIT = 24 * 1024 * 1024
EXPERT_VMEM = 24 * 1024 * 1024
SMALL_VMEM = 12 * 1024 * 1024


def swap(array, axis, bits):
    pairs = [(j, j ^ bits) for j in range(lax.axis_size(axis))]
    return lax.ppermute(array, axis, pairs)


def upward(array, axis, bit):
    pairs = [(j, j ^ bit) for j in range(lax.axis_size(axis)) if not j & bit]
    return lax.ppermute(array, axis, pairs)


def bits_of(axis):
    size = lax.axis_size(axis)
    return [1 << n for n in range(size.bit_length() - 1)]


def spread(piece, axis):
    bits = bits_of(axis)
    pieces = {0: piece}
    for bit in reversed(bits):
        for key in sorted(pieces):
            pieces[key | bit] = swap(pieces[key], axis, bit)
    return [pieces[key] for key in range(1 << len(bits))]


def total(terms):
    return sum(term.astype(jnp.float32) for term in terms).astype(jnp.bfloat16)


def gather_sum(keep, give, axis):
    bits = bits_of(axis)
    got = swap(give, axis, bits[0])
    parts = {2 * n: [keep[n], got[n]] for n in range(keep.shape[0])}
    for bit in bits[1:]:
        keys = [key for key in parts if not key & bit]
        if len(keys) == 1:
            sent = [swap(total(parts[key | bit]), axis, bit) for key in keys]
        else:
            sent = jnp.stack([total(parts[key | bit]) for key in keys])
            sent = swap(sent, axis, bit)
        parts = {key: parts[key] + [sent[n]] for n, key in enumerate(keys)}
    return [keep, got] + parts[0][2:]


def first_rows(terms):
    return [term[0] if term.ndim == 3 else term for term in terms]


def tokens_kernel(experts, base_ref, *refs):
    sources, outs = refs[:4], refs[4:-5]
    x_ref, gain_ref, routes_ref, shares_ref = refs[-5:-1]
    *blocks, mix_ref = outs
    loads = [
        pltpu.make_async_copy(source, target, refs[-1].at[n])
        for n, (source, target) in enumerate(zip(sources, refs[-5:-1]))
    ]
    for load in loads:
        load.start()
    for load in loads:
        load.wait()
    tok_count = x_ref.shape[0]
    rows = mix_ref.shape[2]
    wide = x_ref[...].astype(jnp.float32)
    normed = wide * lax.rsqrt(jnp.mean(wide * wide, axis=-1, keepdims=True) + 1e-06)
    normed = (normed * gain_ref[...]).astype(jnp.bfloat16)
    routes, shares = routes_ref[...], shares_ref[...]
    expert = lax.broadcasted_iota(jnp.int32, (experts, tok_count), 0) ^ base_ref[0]
    named = jnp.zeros((experts, tok_count), jnp.float32)
    share = jnp.zeros((experts, tok_count), jnp.float32)
    for k in range(routes.shape[0]):
        hit = routes[k : k + 1, :] == expert
        named = named + jnp.where(hit, 1.0, 0.0)
        share = share + jnp.where(hit, shares[k : k + 1, :], 0.0)
    row = lax.broadcasted_iota(jnp.int32, (tok_count, tok_count), 0)
    col = lax.broadcasted_iota(jnp.int32, (tok_count, tok_count), 1)
    earlier = jnp.where(row < col, 1.0, 0.0).astype(jnp.bfloat16)
    ranks = jnp.dot(named.astype(jnp.bfloat16), earlier, preferred_element_type=jnp.float32)
    places = jnp.where(named > 0.5, ranks, -1.0)
    slot = lax.broadcasted_iota(jnp.int32, (rows, tok_count), 0).astype(jnp.float32)
    picks = [jnp.where(places[k : k + 1, :] == slot, 1.0, 0.0) for k in range(experts)]
    pick = jnp.concatenate(picks, axis=0).astype(jnp.bfloat16)
    sent = jnp.dot(pick, normed, preferred_element_type=jnp.float32).astype(jnp.bfloat16)
    if len(blocks) == 1:
        blocks[0][...] = sent
    else:
        half = sent.shape[1] // 2
        for k in range(experts):
            for side in range(2):
                part = sent[k * rows : (k + 1) * rows, side * half : (side + 1) * half]
                blocks[k][side * rows : (side + 1) * rows, :] = part
    for k in range(experts):
        mix = picks[k] * share[k : k + 1, :]
        high = mix.astype(jnp.bfloat16)
        mix_ref[0, k] = high
        mix_ref[1, k] = (mix - high.astype(jnp.float32)).astype(jnp.bfloat16)


def route_tokens(base, moe_input, norm_gain, routes, route_weights, experts, capacity, split):
    tok_count, width = moe_input.shape
    operands = [moe_input, norm_gain.reshape(1, -1), routes.T, route_weights.T]
    operands = [pltpu.with_memory_space_constraint(a, pltpu.HBM) for a in operands]
    unit = 4 if split else 8
    rows = -(-capacity // unit) * unit
    if split:
        shapes = [jax.ShapeDtypeStruct((2 * rows, width // 2), jnp.bfloat16)] * experts
    else:
        shapes = [jax.ShapeDtypeStruct((experts * rows, width), jnp.bfloat16)]
    shapes.append(jax.ShapeDtypeStruct((2, experts, rows, tok_count), jnp.bfloat16))
    return pl.pallas_call(
        lambda *refs: tokens_kernel(experts, *refs),
        out_shape=shapes,
        in_specs=[pl.BlockSpec(memory_space=pltpu.SMEM)]
        + [pl.BlockSpec(memory_space=pltpu.HBM)] * 4,
        scratch_shapes=[pltpu.VMEM(a.shape, a.dtype) for a in operands]
        + [pltpu.SemaphoreType.DMA((4,))],
        cost_estimate=pl.CostEstimate(
            flops=3_000_000_000, transcendentals=0, bytes_accessed=4_000_000
        ),
        compiler_params=pltpu.CompilerParams(vmem_limit_bytes=SMALL_VMEM),
    )(base.reshape(1), *operands)


def experts_kernel(count, *refs):
    x_refs = refs[:count]
    gate_ref, up_ref, down_ref, keep_ref, give_ref = refs[count:]
    inner = gate_ref.shape[1]
    width = down_ref.shape[1]
    order = list(range(1, count, 2)) + list(range(0, count, 2))
    x = jnp.concatenate([x_refs[n][...] for n in order], axis=0)
    half = x.shape[0] // 2

    def product(a, b):
        return jnp.dot(a, b, preferred_element_type=jnp.float32)

    hidden = []
    for edge in range(0, inner, 256):
        cols = pl.ds(edge, min(256, inner - edge))
        gate, up = product(x, gate_ref[:, cols]), product(x, up_ref[:, cols])
        hidden.append((gate / (1.0 + jnp.exp(-gate)) * up).astype(jnp.bfloat16))
    hidden = jnp.concatenate(hidden, axis=1)
    for edge in range(0, width, width // 2):
        cols = pl.ds(edge, width // 2)
        part = product(hidden, down_ref[:, cols]).astype(jnp.bfloat16)
        shape = (*give_ref.shape[:2], width // 2)
        give_ref[:, :, cols] = part[:half].reshape(shape)
        keep_ref[:, :, cols] = part[half:].reshape(shape)


def expert_rows(pieces, weights):
    rows, width = pieces[0].shape
    inner = weights[0].shape[1]
    count = len(pieces)
    on_chip = pl.BlockSpec(memory_space=pltpu.VMEM)
    out = jax.ShapeDtypeStruct((count // 2, rows, width), jnp.bfloat16)
    return pl.pallas_call(
        lambda *refs: experts_kernel(count, *refs),
        out_shape=(out, out),
        in_specs=[on_chip] * (count + 3),
        cost_estimate=pl.CostEstimate(
            flops=6 * count * rows * width * inner,
            transcendentals=count * rows * inner,
            bytes_accessed=6 * width * inner,
        ),
        compiler_params=pltpu.CompilerParams(vmem_limit_bytes=EXPERT_VMEM),
    )(*pieces, *weights)


def small_call(kernel, out_shape):
    def call(*operands):
        return pl.pallas_call(
            kernel,
            out_shape=out_shape,
            cost_estimate=pl.CostEstimate(
                flops=1_000_000_000, transcendentals=0, bytes_accessed=1_000_000
            ),
            compiler_params=pltpu.CompilerParams(vmem_limit_bytes=SMALL_VMEM),
        )(*operands)

    return call


def pair_kernel(*refs):
    *blocks, out_ref = refs
    half = blocks[0].shape[1]
    rows = blocks[0].shape[0] // 2
    for side in range(2):
        parts = [ref[side * rows : (side + 1) * rows, :] for ref in blocks]
        out_ref[:, side * half : (side + 1) * half] = jnp.concatenate(parts, axis=0)


def pair(blocks):
    tall, half = blocks[0].shape
    shape = jax.ShapeDtypeStruct((len(blocks) * tall // 2, 2 * half), jnp.bfloat16)
    return small_call(pair_kernel, shape)(*blocks)


def fold_kernel(count, *refs):
    terms, outs = refs[: len(refs) - count], refs[len(refs) - count :]
    rows, half = outs[0].shape[0] // 2, outs[0].shape[1]
    for side in range(2):
        cols = slice(side * half, (side + 1) * half)
        values = [ref[0, :, cols] if len(ref.shape) == 3 else ref[:, cols] for ref in terms]
        summed = sum(value.astype(jnp.float32) for value in values).astype(jnp.bfloat16)
        for n, out_ref in enumerate(outs):
            out_ref[side * rows : (side + 1) * rows, :] = summed[n * rows : (n + 1) * rows]


def fold(terms, count):
    rows, width = terms[0].shape[-2:]
    shape = jax.ShapeDtypeStruct((2 * rows // count, width // 2), jnp.bfloat16)
    return small_call(functools.partial(fold_kernel, count), [shape] * count)(*terms)


def join_kernel(*refs):
    *pieces, out_ref = refs
    start = 0
    for piece in pieces:
        out_ref[start : start + piece.shape[0], :] = piece[...]
        start += piece.shape[0]


def join(pieces):
    count = sum(piece.shape[0] for piece in pieces)
    shape = jax.ShapeDtypeStruct((count, pieces[0].shape[1]), jnp.bfloat16)
    return small_call(join_kernel, shape)(*pieces)


def blend_kernel(keys, started, mix_ref, *refs):
    out_ref = refs[-1]
    rows = mix_ref.shape[2]
    sides = refs[0].shape[0] // rows
    half = refs[0].shape[1]
    for side in range(sides):
        cols = slice(side * half, (side + 1) * half)
        result = refs[-2][:, cols] if started else 0.0
        for key, rows_ref in zip(keys, refs):
            for n in range(2):
                result = result + lax.dot_general(
                    mix_ref[n, key],
                    rows_ref[side * rows : (side + 1) * rows, :],
                    (((0,), (0,)), ((), ())),
                    preferred_element_type=jnp.float32,
                )
        out_ref[:, cols] = result.astype(out_ref.dtype)


def blend(mix, rows, started, final):
    keys = sorted(rows)
    width = rows[keys[0]].size // mix.shape[2]
    operands = [rows[key] for key in keys] + ([] if started is None else [started])
    return pl.pallas_call(
        lambda *refs: blend_kernel(keys, started is not None, *refs),
        out_shape=jax.ShapeDtypeStruct(
            (mix.shape[3], width), jnp.bfloat16 if final else jnp.float32
        ),
        cost_estimate=pl.CostEstimate(
            flops=1_500_000_000, transcendentals=0, bytes_accessed=2_000_000
        ),
        compiler_params=pltpu.CompilerParams(vmem_limit_bytes=SMALL_VMEM),
    )(mix, *operands)


def attend_kernel(scaling, place_ref, q_ref, near_ref, far_ref, spots_ref, mix_ref, gain_ref, w_ref, *outs):
    keep_ref, give_ref = outs
    count = 2 * keep_ref.shape[0]
    rows = keep_ref.shape[1]
    value_dim = gain_ref.shape[1]
    key_dim = near_ref.shape[1] - value_dim
    heads = q_ref.shape[1]
    length = near_ref.shape[0]
    span = length
    while span > 2048 and span % 2 == 0:
        span = span // 2
    order = list(range(1, count, 2)) + list(range(0, count, 2))
    queries, spots = [], []
    for n in order:
        start = (place_ref[1] ^ n) * rows
        queries.append([q_ref[pl.ds(start, rows), head, :] for head in range(heads)])
        spots.append(place_ref[0] + start + lax.broadcasted_iota(jnp.int32, (rows, 1), 0))
    queries = [jnp.concatenate(part, axis=0) for part in zip(*queries)]
    spot = jnp.concatenate(spots, axis=0)
    lane = lax.broadcasted_iota(jnp.int32, (count * rows, key_dim), 1)
    attended = []
    for head in range(heads):
        mapped = []
        for m in range(2):
            chosen = (lane >= m * key_dim // 2) & (lane < (m + 1) * key_dim // 2)
            one = jnp.where(chosen, queries[head], 0.0)
            one = one.astype(jnp.bfloat16)

            def step(n, running, kv_ref, offset, one=one):
                peak, sums, numer = running
                here = pl.ds(n * span, span)
                there = pl.ds(offset + n * span, span)
                scores = lax.dot_general(
                    one,
                    kv_ref[here, :key_dim],
                    (((1,), (1,)), ((), ())),
                    preferred_element_type=jnp.float32,
                )
                visible = spots_ref[:, there] <= spot
                scores = jnp.where(visible, scores * scaling, NEG_LARGE)
                top = jnp.maximum(peak, jnp.max(scores, axis=1, keepdims=True))
                weights = jnp.exp(scores - top)
                factor = jnp.exp(peak - top)
                sums = sums * factor + jnp.sum(weights, axis=1, keepdims=True)
                numer = numer * factor + jnp.dot(
                    weights.astype(jnp.bfloat16),
                    kv_ref[here, key_dim:],
                    preferred_element_type=jnp.float32,
                )
                return top, sums, numer

            state = (
                jnp.full((count * rows, 1), NEG_LARGE, jnp.float32),
                jnp.zeros((count * rows, 1), jnp.float32),
                jnp.zeros((count * rows, value_dim), jnp.float32),
            )
            for kv_ref, offset in ((near_ref, 0), (far_ref, length)):
                if span == length:
                    state = step(0, state, kv_ref, offset)
                else:
                    state = lax.fori_loop(
                        0,
                        length // span,
                        functools.partial(step, kv_ref=kv_ref, offset=offset),
                        state,
                    )
            mapped.append(state[2] / state[1])
        blended = mapped[0] - mix_ref[head] * mapped[1]
        scale = lax.rsqrt(jnp.mean(blended * blended, axis=-1, keepdims=True) + 1e-05)
        attended.append((blended * scale * gain_ref[...]).astype(jnp.bfloat16))
    flat = jnp.concatenate(attended, axis=1)
    part = jnp.dot(flat, w_ref[...], preferred_element_type=jnp.float32).astype(jnp.bfloat16)
    give_ref[...] = part[: count // 2 * rows].reshape(give_ref.shape)
    keep_ref[...] = part[count // 2 * rows :].reshape(keep_ref.shape)


def attend(place, queries, both, spots, mix_scale, head_gain, out_weight, parts, scaling):
    rows_here = queries.shape[0]
    width = out_weight.shape[1]
    out = jax.ShapeDtypeStruct((parts // 2, rows_here // parts, width), jnp.bfloat16)
    small = pl.BlockSpec(memory_space=pltpu.SMEM)
    large = pl.BlockSpec(memory_space=pltpu.VMEM)
    return pl.pallas_call(
        lambda *refs: attend_kernel(scaling, *refs),
        out_shape=(out, out),
        in_specs=[small, large, large, large, large, small, large, large],
        cost_estimate=pl.CostEstimate(
            flops=5_000_000_000, transcendentals=0, bytes_accessed=4_000_000
        ),
        compiler_params=pltpu.CompilerParams(vmem_limit_bytes=VMEM_LIMIT),
    )(place, queries, *both, spots, mix_scale, head_gain.reshape(1, -1), out_weight)


def step(
    queries,
    keys,
    values,
    mix_scale,
    head_gain,
    out_weight,
    moe_input,
    norm_gain,
    routes,
    route_weights,
    gate_weight,
    up_weight,
    down_weight,
):
    rows_here, _, key_dim = queries.shape
    ep_size = lax.axis_size("ep")
    tp_size = lax.axis_size("tp")
    ep_index = lax.axis_index("ep").astype(jnp.int32)
    tp_index = lax.axis_index("tp").astype(jnp.int32)
    tok_count, width = moe_input.shape
    top_count = routes.shape[1]
    experts = ep_size * gate_weight.shape[0]
    capacity = max(2, 3 * top_count * tok_count // (2 * experts))
    split = ep_size <= 8

    both = jnp.concatenate([keys, values], axis=2).reshape(rows_here, -1)
    bits = bits_of("ep")
    held = [both]
    for bit in bits[:-1]:
        held.append(swap(both, "ep", bit))
        both = join(held)
        held = [both]
    both = [both, upward(both, "ep", bits[-1])]

    base = ep_index if split else jnp.zeros_like(ep_index)
    *blocks, mix = route_tokens(
        base, moe_input, norm_gain, routes, route_weights, experts, capacity, split
    )

    weights = [gate_weight[0], up_weight[0], down_weight[0]]
    if split:
        weights = [pltpu.with_memory_space_constraint(w, pltpu.VMEM) for w in weights]

    def expert_group(piece):
        pieces = spread(piece, "tp")
        keep, give = expert_rows(pieces, weights)
        return gather_sum(keep, give, "tp")

    if split:
        arrived = [blocks[0]] + [swap(blocks[k], "ep", k) for k in range(1, ep_size)]
        returned = {}
        for low in range(0, ep_size, 2):
            members = range(low, min(low + 2, ep_size))
            group = pair([arrived[k] for k in members])
            done = fold(expert_group(group), len(members))
            for k, block in zip(members, done):
                returned[k] = swap(block, "ep", k) if k else block
        early = {k: returned[k] for k in range(ep_size - 2)}
        late = {k: returned[k] for k in range(ep_size - 2, ep_size)}
        mixed = blend(mix, early, None, False)
        mixed = blend(mix, late, mixed, True)
    else:
        count = blocks[0].shape[0]

        def exchange(rows):
            rows = rows.reshape(ep_size, -1, width)
            rows = lax.all_to_all(rows, "ep", split_axis=0, concat_axis=0, tiled=True)
            return rows.reshape(count, width)

        back = exchange(total(first_rows(expert_group(exchange(blocks[0])))))
        mixed = blend(mix.reshape(2, 1, count, tok_count), {0: back}, None, True)

    place = jnp.stack([ep_index * rows_here, tp_index])
    length = 2 * both[0].shape[0]
    spots = jnp.arange(length, dtype=jnp.int32)
    spots = ((spots // rows_here) ^ ep_index) * rows_here + spots % rows_here
    keep, give = attend(
        place,
        queries,
        both,
        spots.reshape(1, -1),
        mix_scale,
        head_gain,
        out_weight.reshape(-1, width),
        tp_size,
        1.0 / math.sqrt(key_dim // 2),
    )
    terms = gather_sum(keep, give, "tp")
    attn_out = total(first_rows(terms))
    return attn_out, mixed


def solution(mesh):
    in_specs = (
        P("ep", "tp", None),
        P("ep", "tp", None),
        P("ep", "tp", None),
        P("tp"),
        P(),
        P("tp", None, None),
        P(("ep", "tp"), None),
        P(),
        P(("ep", "tp"), None),
        P(("ep", "tp"), None),
        P("ep", None, "tp"),
        P("ep", None, "tp"),
        P("ep", "tp", None),
    )
    out_specs = (P(("ep", "tp"), None), P(("ep", "tp"), None))
    return jax.shard_map(step, mesh=mesh, in_specs=in_specs, out_specs=out_specs, check_vma=False)
```

profile of v0, /device:TPU:19, one launch (start us, length us, event | category | flops | bytes accessed | tf_op | source)
XLA Modules:
  0.0 138.6 jit_solution(15117096217867659016)
XLA Ops:
  0.6 0.8 maximum_bitcast_fusion.refs_0_
  1.5 1.3 collective-permute-start
  2.8 1.7 %shard_map.143 = (bf16[72,1024]{1,0:T(8,128)(2,1)S(1)}, bf16[72,1024]{1,0:T(8,128)(2,1)S(1)}, bf16[72,1024]{1,0:T(8,128)(2,1)S(1)}, bf16[72,1024]{1,0:T(8,128)(2...) custom-call(s32[1]{0:T(128)} %bitcast.7.refs_0_, ...), custom_call_target="tpu_custom_call" | custom-call | flops 3000000000 | bytes 4000000 | tf_op jit(solution)/shard_map/pallas_call | solution.py:124
  4.4 0.1 collective-permute-start.30
  4.6 2.3 %collective-permute-start.31 = (bf16[72,1024]{1,0:T(8,128)(2,1)S(1)}, bf16[72,1024]{1,0:T(8,128)(2,1)S(1)}, u32[]{:S(2)}, u32[]{:S(2)}) collective-permute-start(bf16[72,1024]{1,0:T(8,128)(2,1)S(1)} %get-tuple-element.51), channel_id=1, source_target_pairs={{0,20},{4,16},{8,28},{12,24},{16,4},{20,0},{24,12},{28,8},{1,21},{... | collective-permute-start | bytes 442376 | tf_op jit(solution)/shard_map/ppermute | solution.py:19
  6.8 1.3 collective-permute-start.21
  8.1 1.1 collective-permute-start.22
  9.3 1.4 collective-permute-start.1
  10.7 2.3 %collective-permute-done.30.refs_0_ = bf16[72,1024]{1,0:T(8,128)(2,1)S(1)} collective-permute-done((bf16[72,1024]{1,0:T(8,128)(2,1)S(1)}, bf16[72,1024]{1,0:T(8,128)(2,1)S(1)}, u32[]{:S(2)}, u32[]{:S(2)}) %collective-permute-start.30) | collective-permute-done | bytes 147488 | tf_op jit(solution)/shard_map/ppermute | solution.py:19
  13.0 3.7 %collective-permute-done.31.refs_1_ = bf16[72,1024]{1,0:T(8,128)(2,1)S(1)} collective-permute-done((bf16[72,1024]{1,0:T(8,128)(2,1)S(1)}, bf16[72,1024]{1,0:T(8,128)(2,1)S(1)}, u32[]{:S(2)}, u32[]{:S(2)}) %collective-permute-start.31) | collective-permute-done | bytes 147488 | tf_op jit(solution)/shard_map/ppermute | solution.py:19
  16.7 0.3 collective-permute-start.33
  17.0 6.4 %collective-permute-done.1.refs_1_ = bf16[384,256]{1,0:T(8,128)(2,1)S(1)} collective-permute-done((bf16[384,256]{1,0:T(8,128)(2,1)S(1)}, bf16[384,256]{1,0:T(8,128)(2,1)S(1)}, u32[]{:S(2)}, u32[]{:S(2)}) %collective-permute-start.1) | collective-permute-done | bytes 196640 | tf_op jit(solution)/shard_map/ppermute | solution.py:19
  23.4 1.3 collective-permute-start.2
  24.7 0.1 pad_add_fusion.refs_0_
  24.8 4.0 %collective-permute-start.5 = (bf16[72,1024]{1,0:T(8,128)(2,1)S(1)}, bf16[72,1024]{1,0:T(8,128)(2,1)S(1)}, u32[]{:S(2)}, u32[]{:S(2)}) collective-permute-start(bf16[72,1024]{1,0:T(8,128)(2,1)S(1)} %get-tuple-element.32), channel_id=1, source_target_pairs={{0,24},{4,28},{8,16},{12,20},{16,8},{20,12},{24,0},{28,4},{1,25},{... | collective-permute-start | bytes 442376 | tf_op jit(solution)/shard_map/ppermute | solution.py:19
  28.8 1.1 collective-permute-start.6
  29.9 3.0 %collective-permute-start.32 = (bf16[72,2048]{1,0:T(8,128)(2,1)S(1)}, bf16[72,2048]{1,0:T(8,128)(2,1)S(1)}, u32[]{:S(2)}, u32[]{:S(2)}) collective-permute-start(bf16[72,2048]{1,0:T(8,128)(2,1)S(1)} %shard_map.153.refs_0_), channel_id=1, source_target_pairs={{0,1},{1,0},{2,3},{3,2},{4,5},{5,4},{6,7},{7,6},{8,9},{9,8},{10,11... | collective-permute-start | bytes 884744 | tf_op jit(solution)/shard_map/ppermute | solution.py:19
  33.0 22.2 %collective-permute-done.5.refs_0_ = bf16[72,1024]{1,0:T(8,128)(2,1)S(1)} collective-permute-done((bf16[72,1024]{1,0:T(8,128)(2,1)S(1)}, bf16[72,1024]{1,0:T(8,128)(2,1)S(1)}, u32[]{:S(2)}, u32[]{:S(2)}) %collective-permute-start.5) | collective-permute-done | bytes 147488 | tf_op jit(solution)/shard_map/ppermute | solution.py:19
  55.2 0.3 collective-permute-start.24
  55.4 3.9 %collective-permute-done.6.refs_1_ = bf16[72,1024]{1,0:T(8,128)(2,1)S(1)} collective-permute-done((bf16[72,1024]{1,0:T(8,128)(2,1)S(1)}, bf16[72,1024]{1,0:T(8,128)(2,1)S(1)}, u32[]{:S(2)}, u32[]{:S(2)}) %collective-permute-start.6) | collective-permute-done | bytes 147488 | tf_op jit(solution)/shard_map/ppermute | solution.py:19
  59.3 0.5 collective-permute-start.23
  59.8 0.3 collective-permute-start.16
  60.1 0.3 collective-permute-start.34
  60.5 4.2 %shard_map.142 = (bf16[2,48,2048]{2,1,0:T(8,128)(2,1)S(1)}, bf16[2,48,2048]{2,1,0:T(8,128)(2,1)S(1)}) custom-call(s32[2]{0:T(128)S(1)} %pad_add_fusion.refs_0_, bf16[192,2,128]{2,1,0:T(2,128)(2,1)S(1)} %copy-done.4, bf16[768,256]{1,0:T(8,128)(2,1)S(1)} %shard_map.141.refs_2_, bf16[768,256]{1,0:T(8,128)(2,1)S(1)} %collective-permute-done.2.refs_3_, ...), custom_call_target="tpu_custom_call" | custom-call | flops 5000000000 | bytes 4000000 | tf_op jit(solution)/shard_map/pallas_call | solution.py:360
  64.7 0.3 collective-permute-start.15
  65.0 1.2 collective-permute-start.8
  66.2 0.6 collective-permute-start.25
  66.8 3.9 %shard_map.154 = (bf16[2,72,2048]{2,1,0:T(8,128)(2,1)S(1)}, bf16[2,72,2048]{2,1,0:T(8,128)(2,1)S(1)}) custom-call(bf16[72,2048]{1,0:T(8,128)(2,1)S(1)} %shard_map.153.refs_0_, bf16[72,2048]{1,0:T(8,128)(2,1)S(1)} %collective-permute-done.32.refs_1_, bf16[72,2048]{1,0:T(8,128)(2,1)S(1)} %collective-permute-done.33.refs_2_, ...), custom_call_target="tpu_custom_call" | custom-call | flops 3170893824 | bytes 11010048 | tf_op jit(solution)/shard_map/pallas_call | solution.py:170
  70.6 0.1 collective-permute-start.7
  70.7 1.2 collective-permute-start.17
  71.9 3.8 %collective-permute-done.8.refs_2_ = bf16[72,2048]{1,0:T(8,128)(2,1)S(1)} collective-permute-done((bf16[72,2048]{1,0:T(8,128)(2,1)S(1)}, bf16[72,2048]{1,0:T(8,128)(2,1)S(1)}, u32[]{:S(2)}, u32[]{:S(2)}) %collective-permute-start.8) | collective-permute-done | bytes 294944 | tf_op jit(solution)/shard_map/ppermute | solution.py:19
  75.8 1.4 %collective-permute-start.9 = (bf16[72,2048]{1,0:T(8,128)(2,1)S(1)}, bf16[72,2048]{1,0:T(8,128)(2,1)S(1)}, u32[]{:S(2)}, u32[]{:S(2)}) collective-permute-start(bf16[72,2048]{1,0:T(8,128)(2,1)S(1)} %collective-permute-done.8.refs_2_), channel_id=1, source_target_pairs={{0,1},{1,0},{2,3},{3,2},{4,5},{5,4},{6,7},{7,6},{8,9},{9,8},{10,11... | collective-permute-start | bytes 884744 | tf_op jit(solution)/shard_map/ppermute | solution.py:19
  77.2 3.8 %shard_map.151 = (bf16[2,72,2048]{2,1,0:T(8,128)(2,1)S(1)}, bf16[2,72,2048]{2,1,0:T(8,128)(2,1)S(1)}) custom-call(bf16[72,2048]{1,0:T(8,128)(2,1)S(1)} %shard_map.150.refs_0_, bf16[72,2048]{1,0:T(8,128)(2,1)S(1)} %collective-permute-done.23.refs_1_, bf16[72,2048]{1,0:T(8,128)(2,1)S(1)} %collective-permute-done.24.refs_2_, ...), custom_call_target="tpu_custom_call" | custom-call | flops 3170893824 | bytes 11010048 | tf_op jit(solution)/shard_map/pallas_call | solution.py:170
  81.1 0.6 collective-permute-start.35
  81.7 0.1 collective-permute-start.26
  81.7 4.0 %shard_map.148 = (bf16[2,72,2048]{2,1,0:T(8,128)(2,1)S(1)}, bf16[2,72,2048]{2,1,0:T(8,128)(2,1)S(1)}) custom-call(bf16[72,2048]{1,0:T(8,128)(2,1)S(1)} %shard_map.147.refs_0_, bf16[72,2048]{1,0:T(8,128)(2,1)S(1)} %collective-permute-done.15.refs_1_, bf16[72,2048]{1,0:T(8,128)(2,1)S(1)} %collective-permute-done.16.refs_2_, ...), custom_call_target="tpu_custom_call" | custom-call | flops 3170893824 | bytes 11010048 | tf_op jit(solution)/shard_map/pallas_call | solution.py:170
  85.8 0.5 collective-permute-start.18
  86.3 3.8 %shard_map.145 = (bf16[2,72,2048]{2,1,0:T(8,128)(2,1)S(1)}, bf16[2,72,2048]{2,1,0:T(8,128)(2,1)S(1)}) custom-call(bf16[72,2048]{1,0:T(8,128)(2,1)S(1)} %shard_map.144.refs_0_, bf16[72,2048]{1,0:T(8,128)(2,1)S(1)} %collective-permute-done.7.refs_1_, bf16[72,2048]{1,0:T(8,128)(2,1)S(1)} %collective-permute-done.8.refs_2_, ...), custom_call_target="tpu_custom_call" | custom-call | flops 3170893824 | bytes 11010048 | tf_op jit(solution)/shard_map/pallas_call | solution.py:170
  90.2 0.1 collective-permute-start.10
  90.3 0.1 fusion.4
  90.4 0.3 collective-permute-start.36
  90.8 1.3 collective-permute-start.27
  92.1 0.3 collective-permute-start.19
  92.4 0.1 fusion.1
  92.5 1.3 collective-permute-start.11
  93.8 0.3 collective-permute-start.4
  94.2 4.4 %collective-permute-done.36.refs_2_ = bf16[72,2048]{1,0:T(8,128)(2,1)S(1)} collective-permute-done((bf16[72,2048]{1,0:T(8,128)(2,1)S(1)}, bf16[72,2048]{1,0:T(8,128)(2,1)S(1)}, u32[]{:S(2)}, u32[]{:S(2)}) %collective-permute-start.36) | collective-permute-done | bytes 294944 | tf_op jit(solution)/shard_map/ppermute | solution.py:19
  98.5 0.1 shard_map.155
  98.7 0.1 collective-permute-start.37
  98.7 6.1 %collective-permute-done.27.refs_2_ = bf16[72,2048]{1,0:T(8,128)(2,1)S(1)} collective-permute-done((bf16[72,2048]{1,0:T(8,128)(2,1)S(1)}, bf16[72,2048]{1,0:T(8,128)(2,1)S(1)}, u32[]{:S(2)}, u32[]{:S(2)}) %collective-permute-start.27) | collective-permute-done | bytes 294944 | tf_op jit(solution)/shard_map/ppermute | solution.py:19
  104.9 0.1 shard_map.152
  105.0 6.2 %collective-permute-done.19.refs_2_ = bf16[72,2048]{1,0:T(8,128)(2,1)S(1)} collective-permute-done((bf16[72,2048]{1,0:T(8,128)(2,1)S(1)}, bf16[72,2048]{1,0:T(8,128)(2,1)S(1)}, u32[]{:S(2)}, u32[]{:S(2)}) %collective-permute-start.19) | collective-permute-done | bytes 294944 | tf_op jit(solution)/shard_map/ppermute | solution.py:19
  111.2 0.1 shard_map.149
  111.3 6.2 %collective-permute-done.11.refs_2_ = bf16[72,2048]{1,0:T(8,128)(2,1)S(1)} collective-permute-done((bf16[72,2048]{1,0:T(8,128)(2,1)S(1)}, bf16[72,2048]{1,0:T(8,128)(2,1)S(1)}, u32[]{:S(2)}, u32[]{:S(2)}) %collective-permute-start.11) | collective-permute-done | bytes 294944 | tf_op jit(solution)/shard_map/ppermute | solution.py:19
  117.5 0.1 shard_map.146
  117.6 4.1 %collective-permute-done.4 = bf16[48,2048]{1,0:T(8,128)(2,1)S(1)} collective-permute-done((bf16[48,2048]{1,0:T(8,128)(2,1)S(1)}, bf16[48,2048]{1,0:T(8,128)(2,1)S(1)}, u32[]{:S(2)}, u32[]{:S(2)}) %collective-permute-start.4) | collective-permute-done | bytes 196640 | tf_op jit(solution)/shard_map/ppermute | solution.py:19
  121.7 1.3 collective-permute-start.20
  123.0 1.4 collective-permute-start.13
  124.4 0.8 fusion
  125.1 3.2 %collective-permute-done.20.refs_2_ = bf16[72,1024]{1,0:T(8,128)(2,1)S(1)} collective-permute-done((bf16[72,1024]{1,0:T(8,128)(2,1)S(1)}, bf16[72,1024]{1,0:T(8,128)(2,1)S(1)}, u32[]{:S(2)}, u32[]{:S(2)}) %collective-permute-start.20) | collective-permute-done | bytes 147488 | tf_op jit(solution)/shard_map/ppermute | solution.py:19
  128.3 1.4 %shard_map.156.refs_3_ = f32[96,2048]{1,0:T(8,128)S(1)} custom-call(bf16[2,8,36,96]{3,2,1,0:T(8,128)(2,1)S(1)} %get-tuple-element.31.refs_0_, bf16[72,1024]{1,0:T(8,128)(2,1)S(1)} %get-tuple-element.42.refs_1_, bf16[72,1024]{1,0:T(8,128)(2,1)S(1)} %collective-permute-done.20.refs_2_, bf16[72,1024]{1,0:T(8,128)(2,1)S(1)} %collective-permute-done.28.refs_3_, ...), custom_call_target="tpu_custom_call" | custom-call | flops 1500000000 | bytes 2000000 | tf_op jit(solution)/shard_map/pallas_call | solution.py:266
  129.7 4.1 %collective-permute-done.12.refs_1_ = bf16[72,1024]{1,0:T(8,128)(2,1)S(1)} collective-permute-done((bf16[72,1024]{1,0:T(8,128)(2,1)S(1)}, bf16[72,1024]{1,0:T(8,128)(2,1)S(1)}, u32[]{:S(2)}, u32[]{:S(2)}) %collective-permute-start.12) | collective-permute-done | bytes 147488 | tf_op jit(solution)/shard_map/ppermute | solution.py:19
  133.8 3.4 %collective-permute-done.13.refs_2_ = bf16[72,1024]{1,0:T(8,128)(2,1)S(1)} collective-permute-done((bf16[72,1024]{1,0:T(8,128)(2,1)S(1)}, bf16[72,1024]{1,0:T(8,128)(2,1)S(1)}, u32[]{:S(2)}, u32[]{:S(2)}) %collective-permute-start.13) | collective-permute-done | bytes 147488 | tf_op jit(solution)/shard_map/ppermute | solution.py:19
  137.2 1.3 shard_map.157
  (55 shorter events, 0.5 us)
Async XLA Ops:
  1.5 7.8 %collective-permute-start = (bf16[192,256]{1,0:T(8,128)(2,1)S(1)}, bf16[192,256]{1,0:T(8,128)(2,1)S(1)}, u32[]{:S(2)}, u32[]{:S(2)}) collective-permute-start(bf16[192,256]{1,0:T(8,128)(2,1)S(1)} %maximum_bitcast_fusion.refs_0_), channel_id=1, source_target_pairs={{0,4},{4,0},{8,12},{12,8},{16,20},{20,16},{24,28},{28,24},{1,5},{5... | collective-permute-start | bytes 294920 | tf_op jit(solution)/shard_map/ppermute | solution.py:19
  4.4 8.5 %collective-permute-start.30 = (bf16[72,1024]{1,0:T(8,128)(2,1)S(1)}, bf16[72,1024]{1,0:T(8,128)(2,1)S(1)}, u32[]{:S(2)}, u32[]{:S(2)}) collective-permute-start(bf16[72,1024]{1,0:T(8,128)(2,1)S(1)} %get-tuple-element.50), channel_id=1, source_target_pairs={{0,16},{4,20},{8,24},{12,28},{16,0},{20,4},{24,8},{28,12},{1,17},{... | collective-permute-start | bytes 442376 | tf_op jit(solution)/shard_map/ppermute | solution.py:19
  4.6 12.1 %collective-permute-start.31 = (bf16[72,1024]{1,0:T(8,128)(2,1)S(1)}, bf16[72,1024]{1,0:T(8,128)(2,1)S(1)}, u32[]{:S(2)}, u32[]{:S(2)}) collective-permute-start(bf16[72,1024]{1,0:T(8,128)(2,1)S(1)} %get-tuple-element.51), channel_id=1, source_target_pairs={{0,20},{4,16},{8,28},{12,24},{16,4},{20,0},{24,12},{28,8},{1,21},{... | collective-permute-start | bytes 442376 | tf_op jit(solution)/shard_map/ppermute | solution.py:19
  6.8 18.0 %collective-permute-start.21 = (bf16[72,1024]{1,0:T(8,128)(2,1)S(1)}, bf16[72,1024]{1,0:T(8,128)(2,1)S(1)}, u32[]{:S(2)}, u32[]{:S(2)}) collective-permute-start(bf16[72,1024]{1,0:T(8,128)(2,1)S(1)} %get-tuple-element.44), channel_id=1, source_target_pairs={{0,8},{4,12},{8,0},{12,4},{16,24},{20,28},{24,16},{28,20},{1,9},{5... | collective-permute-start | bytes 442376 | tf_op jit(solution)/shard_map/ppermute | solution.py:19
  8.1 20.7 %collective-permute-start.22 = (bf16[72,1024]{1,0:T(8,128)(2,1)S(1)}, bf16[72,1024]{1,0:T(8,128)(2,1)S(1)}, u32[]{:S(2)}, u32[]{:S(2)}) collective-permute-start(bf16[72,1024]{1,0:T(8,128)(2,1)S(1)} %get-tuple-element.45), channel_id=1, source_target_pairs={{0,12},{4,8},{8,4},{12,0},{16,28},{20,24},{24,20},{28,16},{1,13},{... | collective-permute-start | bytes 442376 | tf_op jit(solution)/shard_map/ppermute | solution.py:19
  9.3 14.1 %collective-permute-start.1 = (bf16[384,256]{1,0:T(8,128)(2,1)S(1)}, bf16[384,256]{1,0:T(8,128)(2,1)S(1)}, u32[]{:S(2)}, u32[]{:S(2)}) collective-permute-start(bf16[384,256]{1,0:T(8,128)(2,1)S(1)} %shard_map.140.refs_0_), channel_id=1, source_target_pairs={{0,8},{4,12},{8,0},{12,4},{16,24},{20,28},{24,16},{28,20},{1,9},{5... | collective-permute-start | bytes 589832 | tf_op jit(solution)/shard_map/ppermute | solution.py:19
  13.0 17.0 %collective-permute-start.14 = (bf16[72,1024]{1,0:T(8,128)(2,1)S(1)}, bf16[72,1024]{1,0:T(8,128)(2,1)S(1)}, u32[]{:S(2)}, u32[]{:S(2)}) collective-permute-start(bf16[72,1024]{1,0:T(8,128)(2,1)S(1)} %get-tuple-element.39), channel_id=1, source_target_pairs={{0,4},{4,0},{8,12},{12,8},{16,20},{20,16},{24,28},{28,24},{1,5},{5... | collective-permute-start | bytes 442376 | tf_op jit(solution)/shard_map/ppermute | solution.py:19
  16.7 43.1 %collective-permute-start.33 = (bf16[72,2048]{1,0:T(8,128)(2,1)S(1)}, bf16[72,2048]{1,0:T(8,128)(2,1)S(1)}, u32[]{:S(2)}, u32[]{:S(2)}) collective-permute-start(bf16[72,2048]{1,0:T(8,128)(2,1)S(1)} %shard_map.153.refs_0_), channel_id=1, source_target_pairs={{0,2},{1,3},{2,0},{3,1},{4,6},{5,7},{6,4},{7,5},{8,10},{9,11},{10,... | collective-permute-start | bytes 884744 | tf_op jit(solution)/shard_map/ppermute | solution.py:19
  23.4 36.7 %collective-permute-start.2 = (bf16[768,256]{1,0:T(8,128)(2,1)S(1)}, bf16[768,256]{1,0:T(8,128)(2,1)S(1)}, u32[]{:S(2)}, u32[]{:S(2)}) collective-permute-start(bf16[768,256]{1,0:T(8,128)(2,1)S(1)} %shard_map.141.refs_2_), channel_id=1, source_target_pairs={{0,16},{4,20},{8,24},{12,28},{1,17},{5,21},{9,25},{13,29},{2,18},{... | collective-permute-start | bytes 1179656 | tf_op jit(solution)/shard_map/ppermute | solution.py:24
  24.8 30.4 %collective-permute-start.5 = (bf16[72,1024]{1,0:T(8,128)(2,1)S(1)}, bf16[72,1024]{1,0:T(8,128)(2,1)S(1)}, u32[]{:S(2)}, u32[]{:S(2)}) collective-permute-start(bf16[72,1024]{1,0:T(8,128)(2,1)S(1)} %get-tuple-element.32), channel_id=1, source_target_pairs={{0,24},{4,28},{8,16},{12,20},{16,8},{20,12},{24,0},{28,4},{1,25},{... | collective-permute-start | bytes 442376 | tf_op jit(solution)/shard_map/ppermute | solution.py:19
  28.8 30.4 %collective-permute-start.6 = (bf16[72,1024]{1,0:T(8,128)(2,1)S(1)}, bf16[72,1024]{1,0:T(8,128)(2,1)S(1)}, u32[]{:S(2)}, u32[]{:S(2)}) collective-permute-start(bf16[72,1024]{1,0:T(8,128)(2,1)S(1)} %get-tuple-element.33), channel_id=1, source_target_pairs={{0,28},{4,24},{8,20},{12,16},{16,12},{20,8},{24,4},{28,0},{1,29},{... | collective-permute-start | bytes 442376 | tf_op jit(solution)/shard_map/ppermute | solution.py:19
  29.9 34.7 %collective-permute-start.32 = (bf16[72,2048]{1,0:T(8,128)(2,1)S(1)}, bf16[72,2048]{1,0:T(8,128)(2,1)S(1)}, u32[]{:S(2)}, u32[]{:S(2)}) collective-permute-start(bf16[72,2048]{1,0:T(8,128)(2,1)S(1)} %shard_map.153.refs_0_), channel_id=1, source_target_pairs={{0,1},{1,0},{2,3},{3,2},{4,5},{5,4},{6,7},{7,6},{8,9},{9,8},{10,11... | collective-permute-start | bytes 884744 | tf_op jit(solution)/shard_map/ppermute | solution.py:19
  32.9 27.5 %copy-start.3 = (bf16[2,128,2048]{2,1,0:T(8,128)(2,1)S(1)}, bf16[2,128,2048]{2,1,0:T(8,128)(2,1)}, u32[]{:S(2)}) copy-start(bf16[2,128,2048]{2,1,0:T(8,128)(2,1)} %param.18) | copy-start | bytes 3145732
  32.9 27.5 %copy-start.4 = (bf16[192,2,128]{2,1,0:T(2,128)(2,1)S(1)}, bf16[192,2,128]{2,1,0:T(2,128)(2,1)}, u32[]{:S(2)}) copy-start(bf16[192,2,128]{2,1,0:T(2,128)(2,1)} %refs_1_.2) | copy-start | bytes 294916
  32.9 27.5 %copy-start.5 = (f32[2]{0:T(128)S(1)}, f32[2]{0:T(128)}, u32[]{:S(2)}) copy-start(f32[2]{0:T(128)} %refs_5_.1) | copy-start | bytes 28
  32.9 27.5 %copy-start.6 = (f32[128]{0:T(128)S(1)}, f32[128]{0:T(128)}, u32[]{:S(2)}) copy-start(f32[128]{0:T(128)} %param.17) | copy-start | bytes 1540
  55.2 9.8 %collective-permute-start.24 = (bf16[72,2048]{1,0:T(8,128)(2,1)S(1)}, bf16[72,2048]{1,0:T(8,128)(2,1)S(1)}, u32[]{:S(2)}, u32[]{:S(2)}) collective-permute-start(bf16[72,2048]{1,0:T(8,128)(2,1)S(1)} %shard_map.150.refs_0_), channel_id=1, source_target_pairs={{0,2},{1,3},{2,0},{3,1},{4,6},{5,7},{6,4},{7,5},{8,10},{9,11},{10,... | collective-permute-start | bytes 884744 | tf_op jit(solution)/shard_map/ppermute | solution.py:19
  59.3 11.4 %collective-permute-start.23 = (bf16[72,2048]{1,0:T(8,128)(2,1)S(1)}, bf16[72,2048]{1,0:T(8,128)(2,1)S(1)}, u32[]{:S(2)}, u32[]{:S(2)}) collective-permute-start(bf16[72,2048]{1,0:T(8,128)(2,1)S(1)} %shard_map.150.refs_0_), channel_id=1, source_target_pairs={{0,1},{1,0},{2,3},{3,2},{4,5},{5,4},{6,7},{7,6},{8,9},{9,8},{10,11... | collective-permute-start | bytes 884744 | tf_op jit(solution)/shard_map/ppermute | solution.py:19
  59.8 10.9 %collective-permute-start.16 = (bf16[72,2048]{1,0:T(8,128)(2,1)S(1)}, bf16[72,2048]{1,0:T(8,128)(2,1)S(1)}, u32[]{:S(2)}, u32[]{:S(2)}) collective-permute-start(bf16[72,2048]{1,0:T(8,128)(2,1)S(1)} %shard_map.147.refs_0_), channel_id=1, source_target_pairs={{0,2},{1,3},{2,0},{3,1},{4,6},{5,7},{6,4},{7,5},{8,10},{9,11},{10,... | collective-permute-start | bytes 884744 | tf_op jit(solution)/shard_map/ppermute | solution.py:19
  60.1 6.0 %collective-permute-start.34 = (bf16[72,2048]{1,0:T(8,128)(2,1)S(1)}, bf16[72,2048]{1,0:T(8,128)(2,1)S(1)}, u32[]{:S(2)}, u32[]{:S(2)}) collective-permute-start(bf16[72,2048]{1,0:T(8,128)(2,1)S(1)} %collective-permute-done.33.refs_2_), channel_id=1, source_target_pairs={{0,1},{1,0},{2,3},{3,2},{4,5},{5,4},{6,7},{7,6},{8,9},{9,8},{10,11... | collective-permute-start | bytes 884744 | tf_op jit(solution)/shard_map/ppermute | solution.py:19
  60.5 6.3 %copy-start = (bf16[1,2048,896]{2,1,0:T(8,128)(2,1)S(1)}, bf16[1,2048,896]{2,1,0:T(8,128)(2,1)}, u32[]{:S(2)}) copy-start(bf16[1,2048,896]{2,1,0:T(8,128)(2,1)} %param.23) | copy-start | bytes 11010052
  60.5 6.3 %copy-start.1 = (bf16[1,2048,896]{2,1,0:T(8,128)(2,1)S(1)}, bf16[1,2048,896]{2,1,0:T(8,128)(2,1)}, u32[]{:S(2)}) copy-start(bf16[1,2048,896]{2,1,0:T(8,128)(2,1)} %param.24) | copy-start | bytes 11010052
  60.5 6.3 %copy-start.2 = (bf16[1,896,2048]{2,1,0:T(8,128)(2,1)S(1)}, bf16[1,896,2048]{2,1,0:T(8,128)(2,1)}, u32[]{:S(2)}) copy-start(bf16[1,896,2048]{2,1,0:T(8,128)(2,1)} %param.25) | copy-start | bytes 11010052
  64.7 16.4 %collective-permute-start.15 = (bf16[72,2048]{1,0:T(8,128)(2,1)S(1)}, bf16[72,2048]{1,0:T(8,128)(2,1)S(1)}, u32[]{:S(2)}, u32[]{:S(2)}) collective-permute-start(bf16[72,2048]{1,0:T(8,128)(2,1)S(1)} %shard_map.147.refs_0_), channel_id=1, source_target_pairs={{0,1},{1,0},{2,3},{3,2},{4,5},{5,4},{6,7},{7,6},{8,9},{9,8},{10,11... | collective-permute-start | bytes 884744 | tf_op jit(solution)/shard_map/ppermute | solution.py:19
  65.0 10.8 %collective-permute-start.8 = (bf16[72,2048]{1,0:T(8,128)(2,1)S(1)}, bf16[72,2048]{1,0:T(8,128)(2,1)S(1)}, u32[]{:S(2)}, u32[]{:S(2)}) collective-permute-start(bf16[72,2048]{1,0:T(8,128)(2,1)S(1)} %shard_map.144.refs_0_), channel_id=1, source_target_pairs={{0,2},{1,3},{2,0},{3,1},{4,6},{5,7},{6,4},{7,5},{8,10},{9,11},{10,... | collective-permute-start | bytes 884744 | tf_op jit(solution)/shard_map/ppermute | solution.py:19
  66.2 11.0 %collective-permute-start.25 = (bf16[72,2048]{1,0:T(8,128)(2,1)S(1)}, bf16[72,2048]{1,0:T(8,128)(2,1)S(1)}, u32[]{:S(2)}, u32[]{:S(2)}) collective-permute-start(bf16[72,2048]{1,0:T(8,128)(2,1)S(1)} %collective-permute-done.24.refs_2_), channel_id=1, source_target_pairs={{0,1},{1,0},{2,3},{3,2},{4,5},{5,4},{6,7},{7,6},{8,9},{9,8},{10,11... | collective-permute-start | bytes 884744 | tf_op jit(solution)/shard_map/ppermute | solution.py:19
  70.6 15.1 %collective-permute-start.7 = (bf16[72,2048]{1,0:T(8,128)(2,1)S(1)}, bf16[72,2048]{1,0:T(8,128)(2,1)S(1)}, u32[]{:S(2)}, u32[]{:S(2)}) collective-permute-start(bf16[72,2048]{1,0:T(8,128)(2,1)S(1)} %shard_map.144.refs_0_), channel_id=1, source_target_pairs={{0,1},{1,0},{2,3},{3,2},{4,5},{5,4},{6,7},{7,6},{8,9},{9,8},{10,11... | collective-permute-start | bytes 884744 | tf_op jit(solution)/shard_map/ppermute | solution.py:19
  70.7 10.9 %collective-permute-start.17 = (bf16[72,2048]{1,0:T(8,128)(2,1)S(1)}, bf16[72,2048]{1,0:T(8,128)(2,1)S(1)}, u32[]{:S(2)}, u32[]{:S(2)}) collective-permute-start(bf16[72,2048]{1,0:T(8,128)(2,1)S(1)} %collective-permute-done.16.refs_2_), channel_id=1, source_target_pairs={{0,1},{1,0},{2,3},{3,2},{4,5},{5,4},{6,7},{7,6},{8,9},{9,8},{10,11... | collective-permute-start | bytes 884744 | tf_op jit(solution)/shard_map/ppermute | solution.py:19
  75.8 10.5 %collective-permute-start.9 = (bf16[72,2048]{1,0:T(8,128)(2,1)S(1)}, bf16[72,2048]{1,0:T(8,128)(2,1)S(1)}, u32[]{:S(2)}, u32[]{:S(2)}) collective-permute-start(bf16[72,2048]{1,0:T(8,128)(2,1)S(1)} %collective-permute-done.8.refs_2_), channel_id=1, source_target_pairs={{0,1},{1,0},{2,3},{3,2},{4,5},{5,4},{6,7},{7,6},{8,9},{9,8},{10,11... | collective-permute-start | bytes 884744 | tf_op jit(solution)/shard_map/ppermute | solution.py:19
  77.2 16.6 %collective-permute-start.3 = (bf16[2,48,2048]{2,1,0:T(8,128)(2,1)S(1)}, bf16[2,48,2048]{2,1,0:T(8,128)(2,1)S(1)}, u32[]{:S(2)}, u32[]{:S(2)}) collective-permute-start(bf16[2,48,2048]{2,1,0:T(8,128)(2,1)S(1)} %get-tuple-element.30), channel_id=1, source_target_pairs={{0,1},{1,0},{2,3},{3,2},{4,5},{5,4},{6,7},{7,6},{8,9},{9,8},{10,11... | collective-permute-start | bytes 1179656 | tf_op jit(solution)/shard_map/ppermute | solution.py:19
  81.1 9.2 %collective-permute-start.35 = (bf16[2,72,2048]{2,1,0:T(8,128)(2,1)S(1)}, bf16[2,72,2048]{2,1,0:T(8,128)(2,1)S(1)}, u32[]{:S(2)}, u32[]{:S(2)}) collective-permute-start(bf16[2,72,2048]{2,1,0:T(8,128)(2,1)S(1)} %get-tuple-element.53), channel_id=1, source_target_pairs={{0,1},{1,0},{2,3},{3,2},{4,5},{5,4},{6,7},{7,6},{8,9},{9,8},{10,11... | collective-permute-start | bytes 1769480 | tf_op jit(solution)/shard_map/ppermute | solution.py:19
  81.7 9.0 %collective-permute-start.26 = (bf16[2,72,2048]{2,1,0:T(8,128)(2,1)S(1)}, bf16[2,72,2048]{2,1,0:T(8,128)(2,1)S(1)}, u32[]{:S(2)}, u32[]{:S(2)}) collective-permute-start(bf16[2,72,2048]{2,1,0:T(8,128)(2,1)S(1)} %get-tuple-element.47), channel_id=1, source_target_pairs={{0,1},{1,0},{2,3},{3,2},{4,5},{5,4},{6,7},{7,6},{8,9},{9,8},{10,11... | collective-permute-start | bytes 1769480 | tf_op jit(solution)/shard_map/ppermute | solution.py:19
  85.8 6.3 %collective-permute-start.18 = (bf16[2,72,2048]{2,1,0:T(8,128)(2,1)S(1)}, bf16[2,72,2048]{2,1,0:T(8,128)(2,1)S(1)}, u32[]{:S(2)}, u32[]{:S(2)}) collective-permute-start(bf16[2,72,2048]{2,1,0:T(8,128)(2,1)S(1)} %get-tuple-element.41), channel_id=1, source_target_pairs={{0,1},{1,0},{2,3},{3,2},{4,5},{5,4},{6,7},{7,6},{8,9},{9,8},{10,11... | collective-permute-start | bytes 1769480 | tf_op jit(solution)/shard_map/ppermute | solution.py:19
  90.2 2.3 %collective-permute-start.10 = (bf16[2,72,2048]{2,1,0:T(8,128)(2,1)S(1)}, bf16[2,72,2048]{2,1,0:T(8,128)(2,1)S(1)}, u32[]{:S(2)}, u32[]{:S(2)}) collective-permute-start(bf16[2,72,2048]{2,1,0:T(8,128)(2,1)S(1)} %get-tuple-element.35), channel_id=1, source_target_pairs={{0,1},{1,0},{2,3},{3,2},{4,5},{5,4},{6,7},{7,6},{8,9},{9,8},{10,11... | collective-permute-start | bytes 1769480 | tf_op jit(solution)/shard_map/ppermute | solution.py:19
  90.4 8.2 %collective-permute-start.36 = (bf16[72,2048]{1,0:T(8,128)(2,1)S(1)}, bf16[72,2048]{1,0:T(8,128)(2,1)S(1)}, u32[]{:S(2)}, u32[]{:S(2)}) collective-permute-start(bf16[72,2048]{1,0:T(8,128)(2,1)S(1)} %fusion.4), channel_id=1, source_target_pairs={{0,2},{1,3},{2,0},{3,1},{4,6},{5,7},{6,4},{7,5},{8,10},{9,11},{10,... | collective-permute-start | bytes 884744 | tf_op jit(solution)/shard_map/ppermute | solution.py:19
  90.8 14.1 %collective-permute-start.27 = (bf16[72,2048]{1,0:T(8,128)(2,1)S(1)}, bf16[72,2048]{1,0:T(8,128)(2,1)S(1)}, u32[]{:S(2)}, u32[]{:S(2)}) collective-permute-start(bf16[72,2048]{1,0:T(8,128)(2,1)S(1)} %fusion.3), channel_id=1, source_target_pairs={{0,2},{1,3},{2,0},{3,1},{4,6},{5,7},{6,4},{7,5},{8,10},{9,11},{10,... | collective-permute-start | bytes 884744 | tf_op jit(solution)/shard_map/ppermute | solution.py:19
  92.1 19.1 %collective-permute-start.19 = (bf16[72,2048]{1,0:T(8,128)(2,1)S(1)}, bf16[72,2048]{1,0:T(8,128)(2,1)S(1)}, u32[]{:S(2)}, u32[]{:S(2)}) collective-permute-start(bf16[72,2048]{1,0:T(8,128)(2,1)S(1)} %fusion.2), channel_id=1, source_target_pairs={{0,2},{1,3},{2,0},{3,1},{4,6},{5,7},{6,4},{7,5},{8,10},{9,11},{10,... | collective-permute-start | bytes 884744 | tf_op jit(solution)/shard_map/ppermute | solution.py:19
  92.5 25.0 %collective-permute-start.11 = (bf16[72,2048]{1,0:T(8,128)(2,1)S(1)}, bf16[72,2048]{1,0:T(8,128)(2,1)S(1)}, u32[]{:S(2)}, u32[]{:S(2)}) collective-permute-start(bf16[72,2048]{1,0:T(8,128)(2,1)S(1)} %fusion.1), channel_id=1, source_target_pairs={{0,2},{1,3},{2,0},{3,1},{4,6},{5,7},{6,4},{7,5},{8,10},{9,11},{10,... | collective-permute-start | bytes 884744 | tf_op jit(solution)/shard_map/ppermute | solution.py:19
  93.8 27.9 %collective-permute-start.4 = (bf16[48,2048]{1,0:T(8,128)(2,1)S(1)}, bf16[48,2048]{1,0:T(8,128)(2,1)S(1)}, u32[]{:S(2)}, u32[]{:S(2)}) collective-permute-start(bf16[48,2048]{1,0:T(8,128)(2,1)S(1)} %fusion.5), channel_id=1, source_target_pairs={{0,2},{1,3},{2,0},{3,1},{4,6},{5,7},{6,4},{7,5},{8,10},{9,11},{10,... | collective-permute-start | bytes 589832 | tf_op jit(solution)/shard_map/ppermute | solution.py:19
  98.7 24.3 %collective-permute-start.37 = (bf16[72,1024]{1,0:T(8,128)(2,1)S(1)}, bf16[72,1024]{1,0:T(8,128)(2,1)S(1)}, u32[]{:S(2)}, u32[]{:S(2)}) collective-permute-start(bf16[72,1024]{1,0:T(8,128)(2,1)S(1)} %get-tuple-element.54), channel_id=1, source_target_pairs={{0,16},{4,20},{8,24},{12,28},{16,0},{20,4},{24,8},{28,12},{1,17},{... | collective-permute-start | bytes 442376 | tf_op jit(solution)/shard_map/ppermute | solution.py:19
  104.8 18.2 %collective-permute-start.38 = (bf16[72,1024]{1,0:T(8,128)(2,1)S(1)}, bf16[72,1024]{1,0:T(8,128)(2,1)S(1)}, u32[]{:S(2)}, u32[]{:S(2)}) collective-permute-start(bf16[72,1024]{1,0:T(8,128)(2,1)S(1)} %get-tuple-element.55), channel_id=1, source_target_pairs={{0,20},{4,16},{8,28},{12,24},{16,4},{20,0},{24,12},{28,8},{1,21},{... | collective-permute-start | bytes 442376 | tf_op jit(solution)/shard_map/ppermute | solution.py:19
  111.2 13.9 %collective-permute-start.28 = (bf16[72,1024]{1,0:T(8,128)(2,1)S(1)}, bf16[72,1024]{1,0:T(8,128)(2,1)S(1)}, u32[]{:S(2)}, u32[]{:S(2)}) collective-permute-start(bf16[72,1024]{1,0:T(8,128)(2,1)S(1)} %get-tuple-element.48), channel_id=1, source_target_pairs={{0,8},{4,12},{8,0},{12,4},{16,24},{20,28},{24,16},{28,20},{1,9},{5... | collective-permute-start | bytes 442376 | tf_op jit(solution)/shard_map/ppermute | solution.py:19
  117.5 7.6 %collective-permute-start.29 = (bf16[72,1024]{1,0:T(8,128)(2,1)S(1)}, bf16[72,1024]{1,0:T(8,128)(2,1)S(1)}, u32[]{:S(2)}, u32[]{:S(2)}) collective-permute-start(bf16[72,1024]{1,0:T(8,128)(2,1)S(1)} %get-tuple-element.49), channel_id=1, source_target_pairs={{0,12},{4,8},{8,4},{12,0},{16,28},{20,24},{24,20},{28,16},{1,13},{... | collective-permute-start | bytes 442376 | tf_op jit(solution)/shard_map/ppermute | solution.py:19
  121.7 6.6 %collective-permute-start.20 = (bf16[72,1024]{1,0:T(8,128)(2,1)S(1)}, bf16[72,1024]{1,0:T(8,128)(2,1)S(1)}, u32[]{:S(2)}, u32[]{:S(2)}) collective-permute-start(bf16[72,1024]{1,0:T(8,128)(2,1)S(1)} %get-tuple-element.43), channel_id=1, source_target_pairs={{0,4},{4,0},{8,12},{12,8},{16,20},{20,16},{24,28},{28,24},{1,5},{5... | collective-permute-start | bytes 442376 | tf_op jit(solution)/shard_map/ppermute | solution.py:19
  123.0 10.8 %collective-permute-start.12 = (bf16[72,1024]{1,0:T(8,128)(2,1)S(1)}, bf16[72,1024]{1,0:T(8,128)(2,1)S(1)}, u32[]{:S(2)}, u32[]{:S(2)}) collective-permute-start(bf16[72,1024]{1,0:T(8,128)(2,1)S(1)} %get-tuple-element.36), channel_id=1, source_target_pairs={{0,24},{4,28},{8,16},{12,20},{16,8},{20,12},{24,0},{28,4},{1,25},{... | collective-permute-start | bytes 442376 | tf_op jit(solution)/shard_map/ppermute | solution.py:19
  123.0 14.2 %collective-permute-start.13 = (bf16[72,1024]{1,0:T(8,128)(2,1)S(1)}, bf16[72,1024]{1,0:T(8,128)(2,1)S(1)}, u32[]{:S(2)}, u32[]{:S(2)}) collective-permute-start(bf16[72,1024]{1,0:T(8,128)(2,1)S(1)} %get-tuple-element.37), channel_id=1, source_target_pairs={{0,28},{4,24},{8,20},{12,16},{16,12},{20,8},{24,4},{28,0},{1,29},{... | collective-permute-start | bytes 442376 | tf_op jit(solution)/shard_map/ppermute | solution.py:19
where the time goes:
time: 139 us
  waiting for transfers between devices  79.9 us (57%)
  starting transfers between devices  30.8 us (22%)
  Pallas kernels  24.8 us (18%)
  other arithmetic  2.04 us (1%)
    ppermute x38, waiting for transfers between devices, swap(): return lax.ppermute(array, axis, pairs)  79.9 us
    ppermute x38, starting transfers between devices, swap(): return lax.ppermute(array, axis, pairs)  29.5 us
    pallas_call x4, Pallas kernels, expert_rows(): pl.pallas_call(lambda *refs: experts_kernel(count, *refs), out_shape=(out...  15.6 us
    pallas_call x1, Pallas kernels, attend(): pl.pallas_call(lambda *refs: attend_kernel(scaling, *refs), out_shape=(ou...  4.18 us
  transfers between devices with their start and end apart: 39, of which 14 were waited for; matrix products, arithmetic and copies ran while one was open for 1% of the time, Pallas kernels for 17%

commit v1 on v0

--- a/solution.py
+++ b/solution.py
@@ -9,9 +9,13 @@
 from jax.sharding import PartitionSpec as P
 
 NEG_LARGE = -1e30
-VMEM_LIMIT = 24 * 1024 * 1024
-EXPERT_VMEM = 24 * 1024 * 1024
-SMALL_VMEM = 12 * 1024 * 1024
+VMEM_LIMIT = 40 * 1024 * 1024
+
+
+def grant(arrays, factor, base=2):
+    size = sum(a.size * jnp.dtype(a.dtype).itemsize for a in arrays)
+    limit = base * 2**20 + factor * size
+    return pltpu.CompilerParams(vmem_limit_bytes=min(limit, VMEM_LIMIT))
 
 
 def swap(array, axis, bits):
@@ -49,7 +53,8 @@
     for bit in bits[1:]:
         keys = [key for key in parts if not key & bit]
         if len(keys) == 1:
-            sent = [swap(total(parts[key | bit]), axis, bit) for key in keys]
+            sums = [total(parts[key | bit]) for key in keys]
+            sent = [swap(one, axis, bit) for one in sums]
         else:
             sent = jnp.stack([total(parts[key | bit]) for key in keys])
             sent = swap(sent, axis, bit)
@@ -64,7 +69,7 @@
 def tokens_kernel(experts, base_ref, *refs):
     sources, outs = refs[:4], refs[4:-5]
     x_ref, gain_ref, routes_ref, shares_ref = refs[-5:-1]
-    *blocks, mix_ref = outs
+    *blocks, table_ref = outs
     loads = [
         pltpu.make_async_copy(source, target, refs[-1].at[n])
         for n, (source, target) in enumerate(zip(sources, refs[-5:-1]))
@@ -74,7 +79,7 @@
     for load in loads:
         load.wait()
     tok_count = x_ref.shape[0]
-    rows = mix_ref.shape[2]
+    rows = blocks[0].size // (experts // len(blocks) * x_ref.shape[1])
     wide = x_ref[...].astype(jnp.float32)
     normed = wide * lax.rsqrt(jnp.mean(wide * wide, axis=-1, keepdims=True) + 1e-06)
     normed = (normed * gain_ref[...]).astype(jnp.bfloat16)
@@ -103,11 +108,8 @@
             for side in range(2):
                 part = sent[k * rows : (k + 1) * rows, side * half : (side + 1) * half]
                 blocks[k][side * rows : (side + 1) * rows, :] = part
-    for k in range(experts):
-        mix = picks[k] * share[k : k + 1, :]
-        high = mix.astype(jnp.bfloat16)
-        mix_ref[0, k] = high
-        mix_ref[1, k] = (mix - high.astype(jnp.float32)).astype(jnp.bfloat16)
+    table_ref[0] = places
+    table_ref[1] = share
 
 
 def route_tokens(base, moe_input, norm_gain, routes, route_weights, experts, capacity, split):
@@ -120,7 +122,7 @@
         shapes = [jax.ShapeDtypeStruct((2 * rows, width // 2), jnp.bfloat16)] * experts
     else:
         shapes = [jax.ShapeDtypeStruct((experts * rows, width), jnp.bfloat16)]
-    shapes.append(jax.ShapeDtypeStruct((2, experts, rows, tok_count), jnp.bfloat16))
+    shapes.append(jax.ShapeDtypeStruct((2, experts, tok_count), jnp.float32))
     return pl.pallas_call(
         lambda *refs: tokens_kernel(experts, *refs),
         out_shape=shapes,
@@ -131,7 +133,7 @@
         cost_estimate=pl.CostEstimate(
             flops=3_000_000_000, transcendentals=0, bytes_accessed=4_000_000
         ),
-        compiler_params=pltpu.CompilerParams(vmem_limit_bytes=SMALL_VMEM),
+        compiler_params=grant([*operands, *shapes], 3),
     )(base.reshape(1), *operands)
 
 
@@ -161,7 +163,7 @@
         keep_ref[:, :, cols] = part[half:].reshape(shape)
 
 
-def expert_rows(pieces, weights):
+def expert_rows(pieces, weights, resident):
     rows, width = pieces[0].shape
     inner = weights[0].shape[1]
     count = len(pieces)
@@ -176,7 +178,7 @@
             transcendentals=count * rows * inner,
             bytes_accessed=6 * width * inner,
         ),
-        compiler_params=pltpu.CompilerParams(vmem_limit_bytes=EXPERT_VMEM),
+        compiler_params=grant([*pieces, out, out, *([] if resident else weights)], 2),
     )(*pieces, *weights)
 
 
@@ -188,7 +190,7 @@
             cost_estimate=pl.CostEstimate(
                 flops=1_000_000_000, transcendentals=0, bytes_accessed=1_000_000
             ),
-            compiler_params=pltpu.CompilerParams(vmem_limit_bytes=SMALL_VMEM),
+            compiler_params=grant(operands, 2),
         )(*operands)
 
     return call
@@ -240,39 +242,44 @@
     return small_call(join_kernel, shape)(*pieces)
 
 
-def blend_kernel(keys, started, mix_ref, *refs):
+def blend_kernel(keys, count, started, table_ref, *refs):
     out_ref = refs[-1]
-    rows = mix_ref.shape[2]
-    sides = refs[0].shape[0] // rows
+    tok_count, width = out_ref.shape
+    rows = refs[0].size // (count * width)
     half = refs[0].shape[1]
-    for side in range(sides):
+    slot = lax.broadcasted_iota(jnp.int32, (rows, tok_count), 0).astype(jnp.float32)
+    mixes = []
+    for key in keys:
+        parts = [
+            jnp.where(table_ref[0, k : k + 1, :] == slot, table_ref[1, k : k + 1, :], 0.0)
+            for k in range(key, key + count)
+        ]
+        mix = jnp.concatenate(parts, axis=0) if count > 1 else parts[0]
+        high = mix.astype(jnp.bfloat16)
+        mixes.append((high, (mix - high.astype(jnp.float32)).astype(jnp.bfloat16)))
+    for side in range(width // half):
         cols = slice(side * half, (side + 1) * half)
         result = refs[-2][:, cols] if started else 0.0
-        for key, rows_ref in zip(keys, refs):
-            for n in range(2):
+        for pair_of, rows_ref in zip(mixes, refs):
+            here = rows_ref[side * count * rows : (side + 1) * count * rows, :]
+            for mix in pair_of:
                 result = result + lax.dot_general(
-                    mix_ref[n, key],
-                    rows_ref[side * rows : (side + 1) * rows, :],
-                    (((0,), (0,)), ((), ())),
-                    preferred_element_type=jnp.float32,
+                    mix, here, (((0,), (0,)), ((), ())), preferred_element_type=jnp.float32
                 )
         out_ref[:, cols] = result.astype(out_ref.dtype)
 
 
-def blend(mix, rows, started, final):
+def blend(table, rows, count, started, shape, final):
     keys = sorted(rows)
-    width = rows[keys[0]].size // mix.shape[2]
     operands = [rows[key] for key in keys] + ([] if started is None else [started])
     return pl.pallas_call(
-        lambda *refs: blend_kernel(keys, started is not None, *refs),
-        out_shape=jax.ShapeDtypeStruct(
-            (mix.shape[3], width), jnp.bfloat16 if final else jnp.float32
-        ),
+        lambda *refs: blend_kernel(keys, count, started is not None, *refs),
+        out_shape=jax.ShapeDtypeStruct(shape, jnp.bfloat16 if final else jnp.float32),
         cost_estimate=pl.CostEstimate(
             flops=1_500_000_000, transcendentals=0, bytes_accessed=2_000_000
         ),
-        compiler_params=pltpu.CompilerParams(vmem_limit_bytes=SMALL_VMEM),
-    )(mix, *operands)
+        compiler_params=grant([table, *operands], 2, 3),
+    )(table, *operands)
 
 
 def attend_kernel(scaling, place_ref, q_ref, near_ref, far_ref, spots_ref, mix_ref, gain_ref, w_ref, *outs):
@@ -364,7 +371,7 @@
         cost_estimate=pl.CostEstimate(
             flops=5_000_000_000, transcendentals=0, bytes_accessed=4_000_000
         ),
-        compiler_params=pltpu.CompilerParams(vmem_limit_bytes=VMEM_LIMIT),
+        compiler_params=grant([queries, out_weight, out, out, *both], 2, 8),
     )(place, queries, *both, spots, mix_scale, head_gain.reshape(1, -1), out_weight)
 
 
@@ -404,7 +411,7 @@
     both = [both, upward(both, "ep", bits[-1])]
 
     base = ep_index if split else jnp.zeros_like(ep_index)
-    *blocks, mix = route_tokens(
+    *blocks, table = route_tokens(
         base, moe_input, norm_gain, routes, route_weights, experts, capacity, split
     )
 
@@ -414,7 +421,7 @@
 
     def expert_group(piece):
         pieces = spread(piece, "tp")
-        keep, give = expert_rows(pieces, weights)
+        keep, give = expert_rows(pieces, weights, split)
         return gather_sum(keep, give, "tp")
 
     if split:
@@ -428,8 +435,9 @@
                 returned[k] = swap(block, "ep", k) if k else block
         early = {k: returned[k] for k in range(ep_size - 2)}
         late = {k: returned[k] for k in range(ep_size - 2, ep_size)}
-        mixed = blend(mix, early, None, False)
-        mixed = blend(mix, late, mixed, True)
+        shape = moe_input.shape
+        mixed = blend(table, early, 1, None, shape, False)
+        mixed = blend(table, late, 1, mixed, shape, True)
     else:
         count = blocks[0].shape[0]
 
@@ -439,7 +447,7 @@
             return rows.reshape(count, width)
 
         back = exchange(total(first_rows(expert_group(exchange(blocks[0])))))
-        mixed = blend(mix.reshape(2, 1, count, tok_count), {0: back}, None, True)
+        mixed = blend(table, {0: back}, experts, None, moe_input.shape, True)
 
     place = jnp.stack([ep_index * rows_here, tp_index])
     length = 2 * both[0].shape[0]

time: 139 us -> 139 us (level)
  no operation moved by 1% of the time
where the time goes in v1:
time: 139 us
  waiting for transfers between devices  79.9 us (57%)
  starting transfers between devices  30.9 us (22%)
  Pallas kernels  24.8 us (18%)
  other arithmetic  2.03 us (1%)
    ppermute x38, waiting for transfers between devices, swap(): return lax.ppermute(array, axis, pairs)  79.9 us
    ppermute x38, starting transfers between devices, swap(): return lax.ppermute(array, axis, pairs)  29.6 us
    pallas_call x4, Pallas kernels, expert_rows(): pl.pallas_call(lambda *refs: experts_kernel(count, *refs), out_shape=(out...  15.5 us
    pallas_call x1, Pallas kernels, attend(): pl.pallas_call(lambda *refs: attend_kernel(scaling, *refs), out_shape=(ou...  4.18 us
  transfers between devices with their start and end apart: 39, of which 14 were waited for; matrix products, arithmetic and copies ran while one was open for 1% of the time, Pallas kernels for 17%

profile of v1, /device:TPU:19, one launch (start us, length us, event | category | flops | bytes accessed | tf_op | source)
XLA Modules:
  0.0 138.5 jit_solution(6408211262213752967)
XLA Ops:
  0.6 0.8 maximum_bitcast_fusion.refs_0_
  1.5 1.3 collective-permute-start
  2.8 1.6 %shard_map.143 = (bf16[72,1024]{1,0:T(8,128)(2,1)S(1)}, bf16[72,1024]{1,0:T(8,128)(2,1)S(1)}, bf16[72,1024]{1,0:T(8,128)(2,1)S(1)}, bf16[72,1024]{1,0:T(8,128)(2...) custom-call(s32[1]{0:T(128)} %bitcast.7.refs_0_, ...), custom_call_target="tpu_custom_call" | custom-call | flops 3000000000 | bytes 4000000 | tf_op jit(solution)/shard_map/pallas_call | solution.py:126
  4.4 0.1 collective-permute-start.30
  4.6 2.2 %collective-permute-start.31 = (bf16[72,1024]{1,0:T(8,128)(2,1)S(1)}, bf16[72,1024]{1,0:T(8,128)(2,1)S(1)}, u32[]{:S(2)}, u32[]{:S(2)}) collective-permute-start(bf16[72,1024]{1,0:T(8,128)(2,1)S(1)} %get-tuple-element.51), channel_id=1, source_target_pairs={{0,20},{4,16},{8,28},{12,24},{16,4},{20,0},{24,12},{28,8},{1,21},{... | collective-permute-start | bytes 442376 | tf_op jit(solution)/shard_map/ppermute | solution.py:23
  6.8 1.3 collective-permute-start.21
  8.1 1.1 collective-permute-start.22
  9.2 1.4 collective-permute-start.1
  10.6 2.3 %collective-permute-done.30.refs_0_ = bf16[72,1024]{1,0:T(8,128)(2,1)S(1)} collective-permute-done((bf16[72,1024]{1,0:T(8,128)(2,1)S(1)}, bf16[72,1024]{1,0:T(8,128)(2,1)S(1)}, u32[]{:S(2)}, u32[]{:S(2)}) %collective-permute-start.30) | collective-permute-done | bytes 147488 | tf_op jit(solution)/shard_map/ppermute | solution.py:23
  13.0 3.7 %collective-permute-done.31.refs_1_ = bf16[72,1024]{1,0:T(8,128)(2,1)S(1)} collective-permute-done((bf16[72,1024]{1,0:T(8,128)(2,1)S(1)}, bf16[72,1024]{1,0:T(8,128)(2,1)S(1)}, u32[]{:S(2)}, u32[]{:S(2)}) %collective-permute-start.31) | collective-permute-done | bytes 147488 | tf_op jit(solution)/shard_map/ppermute | solution.py:23
  16.7 0.3 collective-permute-start.33
  17.0 6.4 %collective-permute-done.1.refs_1_ = bf16[384,256]{1,0:T(8,128)(2,1)S(1)} collective-permute-done((bf16[384,256]{1,0:T(8,128)(2,1)S(1)}, bf16[384,256]{1,0:T(8,128)(2,1)S(1)}, u32[]{:S(2)}, u32[]{:S(2)}) %collective-permute-start.1) | collective-permute-done | bytes 196640 | tf_op jit(solution)/shard_map/ppermute | solution.py:23
  23.4 1.3 collective-permute-start.2
  24.7 0.1 pad_add_fusion.refs_0_
  24.8 4.0 %collective-permute-start.5 = (bf16[72,1024]{1,0:T(8,128)(2,1)S(1)}, bf16[72,1024]{1,0:T(8,128)(2,1)S(1)}, u32[]{:S(2)}, u32[]{:S(2)}) collective-permute-start(bf16[72,1024]{1,0:T(8,128)(2,1)S(1)} %get-tuple-element.32), channel_id=1, source_target_pairs={{0,24},{4,28},{8,16},{12,20},{16,8},{20,12},{24,0},{28,4},{1,25},{... | collective-permute-start | bytes 442376 | tf_op jit(solution)/shard_map/ppermute | solution.py:23
  28.8 1.0 collective-permute-start.6
  29.9 3.0 %collective-permute-start.32 = (bf16[72,2048]{1,0:T(8,128)(2,1)S(1)}, bf16[72,2048]{1,0:T(8,128)(2,1)S(1)}, u32[]{:S(2)}, u32[]{:S(2)}) collective-permute-start(bf16[72,2048]{1,0:T(8,128)(2,1)S(1)} %shard_map.153.refs_0_), channel_id=1, source_target_pairs={{0,1},{1,0},{2,3},{3,2},{4,5},{5,4},{6,7},{7,6},{8,9},{9,8},{10,11... | collective-permute-start | bytes 884744 | tf_op jit(solution)/shard_map/ppermute | solution.py:23
  33.0 22.2 %collective-permute-done.5.refs_0_ = bf16[72,1024]{1,0:T(8,128)(2,1)S(1)} collective-permute-done((bf16[72,1024]{1,0:T(8,128)(2,1)S(1)}, bf16[72,1024]{1,0:T(8,128)(2,1)S(1)}, u32[]{:S(2)}, u32[]{:S(2)}) %collective-permute-start.5) | collective-permute-done | bytes 147488 | tf_op jit(solution)/shard_map/ppermute | solution.py:23
  55.1 0.3 collective-permute-start.24
  55.4 3.9 %collective-permute-done.6.refs_1_ = bf16[72,1024]{1,0:T(8,128)(2,1)S(1)} collective-permute-done((bf16[72,1024]{1,0:T(8,128)(2,1)S(1)}, bf16[72,1024]{1,0:T(8,128)(2,1)S(1)}, u32[]{:S(2)}, u32[]{:S(2)}) %collective-permute-start.6) | collective-permute-done | bytes 147488 | tf_op jit(solution)/shard_map/ppermute | solution.py:23
  59.3 0.5 collective-permute-start.23
  59.8 0.3 collective-permute-start.16
  60.1 0.3 collective-permute-start.34
  60.5 4.2 %shard_map.142 = (bf16[2,48,2048]{2,1,0:T(8,128)(2,1)S(1)}, bf16[2,48,2048]{2,1,0:T(8,128)(2,1)S(1)}) custom-call(s32[2]{0:T(128)S(1)} %pad_add_fusion.refs_0_, bf16[192,2,128]{2,1,0:T(2,128)(2,1)S(1)} %copy-done.4, bf16[768,256]{1,0:T(8,128)(2,1)S(1)} %shard_map.141.refs_2_, bf16[768,256]{1,0:T(8,128)(2,1)S(1)} %collective-permute-done.2.refs_3_, ...), custom_call_target="tpu_custom_call" | custom-call | flops 5000000000 | bytes 4000000 | tf_op jit(solution)/shard_map/pallas_call | solution.py:367
  64.7 0.3 collective-permute-start.15
  65.0 1.2 collective-permute-start.8
  66.2 0.6 collective-permute-start.25
  66.8 3.8 %shard_map.154 = (bf16[2,72,2048]{2,1,0:T(8,128)(2,1)S(1)}, bf16[2,72,2048]{2,1,0:T(8,128)(2,1)S(1)}) custom-call(bf16[72,2048]{1,0:T(8,128)(2,1)S(1)} %shard_map.153.refs_0_, bf16[72,2048]{1,0:T(8,128)(2,1)S(1)} %collective-permute-done.32.refs_1_, bf16[72,2048]{1,0:T(8,128)(2,1)S(1)} %collective-permute-done.33.refs_2_, ...), custom_call_target="tpu_custom_call" | custom-call | flops 3170893824 | bytes 11010048 | tf_op jit(solution)/shard_map/pallas_call | solution.py:172
  70.6 0.1 collective-permute-start.7
  70.7 1.2 collective-permute-start.17
  71.9 3.8 %collective-permute-done.8.refs_2_ = bf16[72,2048]{1,0:T(8,128)(2,1)S(1)} collective-permute-done((bf16[72,2048]{1,0:T(8,128)(2,1)S(1)}, bf16[72,2048]{1,0:T(8,128)(2,1)S(1)}, u32[]{:S(2)}, u32[]{:S(2)}) %collective-permute-start.8) | collective-permute-done | bytes 294944 | tf_op jit(solution)/shard_map/ppermute | solution.py:23
  75.8 1.4 %collective-permute-start.9 = (bf16[72,2048]{1,0:T(8,128)(2,1)S(1)}, bf16[72,2048]{1,0:T(8,128)(2,1)S(1)}, u32[]{:S(2)}, u32[]{:S(2)}) collective-permute-start(bf16[72,2048]{1,0:T(8,128)(2,1)S(1)} %collective-permute-done.8.refs_2_), channel_id=1, source_target_pairs={{0,1},{1,0},{2,3},{3,2},{4,5},{5,4},{6,7},{7,6},{8,9},{9,8},{10,11... | collective-permute-start | bytes 884744 | tf_op jit(solution)/shard_map/ppermute | solution.py:23
  77.2 3.8 %shard_map.151 = (bf16[2,72,2048]{2,1,0:T(8,128)(2,1)S(1)}, bf16[2,72,2048]{2,1,0:T(8,128)(2,1)S(1)}) custom-call(bf16[72,2048]{1,0:T(8,128)(2,1)S(1)} %shard_map.150.refs_0_, bf16[72,2048]{1,0:T(8,128)(2,1)S(1)} %collective-permute-done.23.refs_1_, bf16[72,2048]{1,0:T(8,128)(2,1)S(1)} %collective-permute-done.24.refs_2_, ...), custom_call_target="tpu_custom_call" | custom-call | flops 3170893824 | bytes 11010048 | tf_op jit(solution)/shard_map/pallas_call | solution.py:172
  81.1 0.6 collective-permute-start.35
  81.6 0.1 collective-permute-start.26
  81.7 4.0 %shard_map.148 = (bf16[2,72,2048]{2,1,0:T(8,128)(2,1)S(1)}, bf16[2,72,2048]{2,1,0:T(8,128)(2,1)S(1)}) custom-call(bf16[72,2048]{1,0:T(8,128)(2,1)S(1)} %shard_map.147.refs_0_, bf16[72,2048]{1,0:T(8,128)(2,1)S(1)} %collective-permute-done.15.refs_1_, bf16[72,2048]{1,0:T(8,128)(2,1)S(1)} %collective-permute-done.16.refs_2_, ...), custom_call_target="tpu_custom_call" | custom-call | flops 3170893824 | bytes 11010048 | tf_op jit(solution)/shard_map/pallas_call | solution.py:172
  85.8 0.5 collective-permute-start.18
  86.3 3.8 %shard_map.145 = (bf16[2,72,2048]{2,1,0:T(8,128)(2,1)S(1)}, bf16[2,72,2048]{2,1,0:T(8,128)(2,1)S(1)}) custom-call(bf16[72,2048]{1,0:T(8,128)(2,1)S(1)} %shard_map.144.refs_0_, bf16[72,2048]{1,0:T(8,128)(2,1)S(1)} %collective-permute-done.7.refs_1_, bf16[72,2048]{1,0:T(8,128)(2,1)S(1)} %collective-permute-done.8.refs_2_, ...), custom_call_target="tpu_custom_call" | custom-call | flops 3170893824 | bytes 11010048 | tf_op jit(solution)/shard_map/pallas_call | solution.py:172
  90.1 0.1 collective-permute-start.10
  90.3 0.3 collective-permute-start.36
  90.7 0.1 fusion.3
  90.7 1.3 collective-permute-start.27
  92.0 0.1 fusion.2
  92.1 0.3 collective-permute-start.19
  92.5 1.3 collective-permute-start.11
  93.8 0.3 collective-permute-start.4
  94.1 4.4 %collective-permute-done.36.refs_2_ = bf16[72,2048]{1,0:T(8,128)(2,1)S(1)} collective-permute-done((bf16[72,2048]{1,0:T(8,128)(2,1)S(1)}, bf16[72,2048]{1,0:T(8,128)(2,1)S(1)}, u32[]{:S(2)}, u32[]{:S(2)}) %collective-permute-start.36) | collective-permute-done | bytes 294944 | tf_op jit(solution)/shard_map/ppermute | solution.py:23
  98.5 0.1 shard_map.155
  98.7 0.1 collective-permute-start.37
  98.7 6.1 %collective-permute-done.27.refs_2_ = bf16[72,2048]{1,0:T(8,128)(2,1)S(1)} collective-permute-done((bf16[72,2048]{1,0:T(8,128)(2,1)S(1)}, bf16[72,2048]{1,0:T(8,128)(2,1)S(1)}, u32[]{:S(2)}, u32[]{:S(2)}) %collective-permute-start.27) | collective-permute-done | bytes 294944 | tf_op jit(solution)/shard_map/ppermute | solution.py:23
  104.8 0.1 shard_map.152
  105.0 6.2 %collective-permute-done.19.refs_2_ = bf16[72,2048]{1,0:T(8,128)(2,1)S(1)} collective-permute-done((bf16[72,2048]{1,0:T(8,128)(2,1)S(1)}, bf16[72,2048]{1,0:T(8,128)(2,1)S(1)}, u32[]{:S(2)}, u32[]{:S(2)}) %collective-permute-start.19) | collective-permute-done | bytes 294944 | tf_op jit(solution)/shard_map/ppermute | solution.py:23
  111.2 0.1 shard_map.149
  111.3 6.2 %collective-permute-done.11.refs_2_ = bf16[72,2048]{1,0:T(8,128)(2,1)S(1)} collective-permute-done((bf16[72,2048]{1,0:T(8,128)(2,1)S(1)}, bf16[72,2048]{1,0:T(8,128)(2,1)S(1)}, u32[]{:S(2)}, u32[]{:S(2)}) %collective-permute-start.11) | collective-permute-done | bytes 294944 | tf_op jit(solution)/shard_map/ppermute | solution.py:23
  117.5 0.1 shard_map.146
  117.6 4.1 %collective-permute-done.4 = bf16[48,2048]{1,0:T(8,128)(2,1)S(1)} collective-permute-done((bf16[48,2048]{1,0:T(8,128)(2,1)S(1)}, bf16[48,2048]{1,0:T(8,128)(2,1)S(1)}, u32[]{:S(2)}, u32[]{:S(2)}) %collective-permute-start.4) | collective-permute-done | bytes 196640 | tf_op jit(solution)/shard_map/ppermute | solution.py:23
  121.7 1.3 collective-permute-start.20
  123.0 1.4 collective-permute-start.13
  124.4 0.8 fusion
  125.1 3.2 %collective-permute-done.20.refs_2_ = bf16[72,1024]{1,0:T(8,128)(2,1)S(1)} collective-permute-done((bf16[72,1024]{1,0:T(8,128)(2,1)S(1)}, bf16[72,1024]{1,0:T(8,128)(2,1)S(1)}, u32[]{:S(2)}, u32[]{:S(2)}) %collective-permute-start.20) | collective-permute-done | bytes 147488 | tf_op jit(solution)/shard_map/ppermute | solution.py:23
  128.3 1.4 %shard_map.156.refs_3_ = f32[96,2048]{1,0:T(8,128)S(1)} custom-call(f32[2,8,96]{2,1,0:T(8,128)S(1)} %get-tuple-element.31.refs_0_, bf16[72,1024]{1,0:T(8,128)(2,1)S(1)} %get-tuple-element.42.refs_1_, bf16[72,1024]{1,0:T(8,128)(2,1)S(1)} %collective-permute-done.20.refs_2_, bf16[72,1024]{1,0:T(8,128)(2,1)S(1)} %collective-permute-done.28.refs_3_, ...), custom_call_target="tpu_custom_call" | custom-call | flops 1500000000 | bytes 2000000 | tf_op jit(solution)/shard_map/pallas_call | solution.py:275
  129.7 4.0 %collective-permute-done.12.refs_1_ = bf16[72,1024]{1,0:T(8,128)(2,1)S(1)} collective-permute-done((bf16[72,1024]{1,0:T(8,128)(2,1)S(1)}, bf16[72,1024]{1,0:T(8,128)(2,1)S(1)}, u32[]{:S(2)}, u32[]{:S(2)}) %collective-permute-start.12) | collective-permute-done | bytes 147488 | tf_op jit(solution)/shard_map/ppermute | solution.py:23
  133.7 3.5 %collective-permute-done.13.refs_2_ = bf16[72,1024]{1,0:T(8,128)(2,1)S(1)} collective-permute-done((bf16[72,1024]{1,0:T(8,128)(2,1)S(1)}, bf16[72,1024]{1,0:T(8,128)(2,1)S(1)}, u32[]{:S(2)}, u32[]{:S(2)}) %collective-permute-start.13) | collective-permute-done | bytes 147488 | tf_op jit(solution)/shard_map/ppermute | solution.py:23
  137.2 1.3 shard_map.157
  (55 shorter events, 0.5 us)
Async XLA Ops:
  1.5 7.8 %collective-permute-start = (bf16[192,256]{1,0:T(8,128)(2,1)S(1)}, bf16[192,256]{1,0:T(8,128)(2,1)S(1)}, u32[]{:S(2)}, u32[]{:S(2)}) collective-permute-start(bf16[192,256]{1,0:T(8,128)(2,1)S(1)} %maximum_bitcast_fusion.refs_0_), channel_id=1, source_target_pairs={{0,4},{4,0},{8,12},{12,8},{16,20},{20,16},{24,28},{28,24},{1,5},{5... | collective-permute-start | bytes 294920 | tf_op jit(solution)/shard_map/ppermute | solution.py:23
  4.4 8.5 %collective-permute-start.30 = (bf16[72,1024]{1,0:T(8,128)(2,1)S(1)}, bf16[72,1024]{1,0:T(8,128)(2,1)S(1)}, u32[]{:S(2)}, u32[]{:S(2)}) collective-permute-start(bf16[72,1024]{1,0:T(8,128)(2,1)S(1)} %get-tuple-element.50), channel_id=1, source_target_pairs={{0,16},{4,20},{8,24},{12,28},{16,0},{20,4},{24,8},{28,12},{1,17},{... | collective-permute-start | bytes 442376 | tf_op jit(solution)/shard_map/ppermute | solution.py:23
  4.6 12.1 %collective-permute-start.31 = (bf16[72,1024]{1,0:T(8,128)(2,1)S(1)}, bf16[72,1024]{1,0:T(8,128)(2,1)S(1)}, u32[]{:S(2)}, u32[]{:S(2)}) collective-permute-start(bf16[72,1024]{1,0:T(8,128)(2,1)S(1)} %get-tuple-element.51), channel_id=1, source_target_pairs={{0,20},{4,16},{8,28},{12,24},{16,4},{20,0},{24,12},{28,8},{1,21},{... | collective-permute-start | bytes 442376 | tf_op jit(solution)/shard_map/ppermute | solution.py:23
  6.8 18.0 %collective-permute-start.21 = (bf16[72,1024]{1,0:T(8,128)(2,1)S(1)}, bf16[72,1024]{1,0:T(8,128)(2,1)S(1)}, u32[]{:S(2)}, u32[]{:S(2)}) collective-permute-start(bf16[72,1024]{1,0:T(8,128)(2,1)S(1)} %get-tuple-element.44), channel_id=1, source_target_pairs={{0,8},{4,12},{8,0},{12,4},{16,24},{20,28},{24,16},{28,20},{1,9},{5... | collective-permute-start | bytes 442376 | tf_op jit(solution)/shard_map/ppermute | solution.py:23
  8.1 20.7 %collective-permute-start.22 = (bf16[72,1024]{1,0:T(8,128)(2,1)S(1)}, bf16[72,1024]{1,0:T(8,128)(2,1)S(1)}, u32[]{:S(2)}, u32[]{:S(2)}) collective-permute-start(bf16[72,1024]{1,0:T(8,128)(2,1)S(1)} %get-tuple-element.45), channel_id=1, source_target_pairs={{0,12},{4,8},{8,4},{12,0},{16,28},{20,24},{24,20},{28,16},{1,13},{... | collective-permute-start | bytes 442376 | tf_op jit(solution)/shard_map/ppermute | solution.py:23
  9.2 14.1 %collective-permute-start.1 = (bf16[384,256]{1,0:T(8,128)(2,1)S(1)}, bf16[384,256]{1,0:T(8,128)(2,1)S(1)}, u32[]{:S(2)}, u32[]{:S(2)}) collective-permute-start(bf16[384,256]{1,0:T(8,128)(2,1)S(1)} %shard_map.140.refs_0_), channel_id=1, source_target_pairs={{0,8},{4,12},{8,0},{12,4},{16,24},{20,28},{24,16},{28,20},{1,9},{5... | collective-permute-start | bytes 589832 | tf_op jit(solution)/shard_map/ppermute | solution.py:23
  13.0 16.9 %collective-permute-start.14 = (bf16[72,1024]{1,0:T(8,128)(2,1)S(1)}, bf16[72,1024]{1,0:T(8,128)(2,1)S(1)}, u32[]{:S(2)}, u32[]{:S(2)}) collective-permute-start(bf16[72,1024]{1,0:T(8,128)(2,1)S(1)} %get-tuple-element.39), channel_id=1, source_target_pairs={{0,4},{4,0},{8,12},{12,8},{16,20},{20,16},{24,28},{28,24},{1,5},{5... | collective-permute-start | bytes 442376 | tf_op jit(solution)/shard_map/ppermute | solution.py:23
  16.7 43.1 %collective-permute-start.33 = (bf16[72,2048]{1,0:T(8,128)(2,1)S(1)}, bf16[72,2048]{1,0:T(8,128)(2,1)S(1)}, u32[]{:S(2)}, u32[]{:S(2)}) collective-permute-start(bf16[72,2048]{1,0:T(8,128)(2,1)S(1)} %shard_map.153.refs_0_), channel_id=1, source_target_pairs={{0,2},{1,3},{2,0},{3,1},{4,6},{5,7},{6,4},{7,5},{8,10},{9,11},{10,... | collective-permute-start | bytes 884744 | tf_op jit(solution)/shard_map/ppermute | solution.py:23
  23.4 36.7 %collective-permute-start.2 = (bf16[768,256]{1,0:T(8,128)(2,1)S(1)}, bf16[768,256]{1,0:T(8,128)(2,1)S(1)}, u32[]{:S(2)}, u32[]{:S(2)}) collective-permute-start(bf16[768,256]{1,0:T(8,128)(2,1)S(1)} %shard_map.141.refs_2_), channel_id=1, source_target_pairs={{0,16},{4,20},{8,24},{12,28},{1,17},{5,21},{9,25},{13,29},{2,18},{... | collective-permute-start | bytes 1179656 | tf_op jit(solution)/shard_map/ppermute | solution.py:28
  24.8 30.4 %collective-permute-start.5 = (bf16[72,1024]{1,0:T(8,128)(2,1)S(1)}, bf16[72,1024]{1,0:T(8,128)(2,1)S(1)}, u32[]{:S(2)}, u32[]{:S(2)}) collective-permute-start(bf16[72,1024]{1,0:T(8,128)(2,1)S(1)} %get-tuple-element.32), channel_id=1, source_target_pairs={{0,24},{4,28},{8,16},{12,20},{16,8},{20,12},{24,0},{28,4},{1,25},{... | collective-permute-start | bytes 442376 | tf_op jit(solution)/shard_map/ppermute | solution.py:23
  28.8 30.4 %collective-permute-start.6 = (bf16[72,1024]{1,0:T(8,128)(2,1)S(1)}, bf16[72,1024]{1,0:T(8,128)(2,1)S(1)}, u32[]{:S(2)}, u32[]{:S(2)}) collective-permute-start(bf16[72,1024]{1,0:T(8,128)(2,1)S(1)} %get-tuple-element.33), channel_id=1, source_target_pairs={{0,28},{4,24},{8,20},{12,16},{16,12},{20,8},{24,4},{28,0},{1,29},{... | collective-permute-start | bytes 442376 | tf_op jit(solution)/shard_map/ppermute | solution.py:23
  29.9 34.7 %collective-permute-start.32 = (bf16[72,2048]{1,0:T(8,128)(2,1)S(1)}, bf16[72,2048]{1,0:T(8,128)(2,1)S(1)}, u32[]{:S(2)}, u32[]{:S(2)}) collective-permute-start(bf16[72,2048]{1,0:T(8,128)(2,1)S(1)} %shard_map.153.refs_0_), channel_id=1, source_target_pairs={{0,1},{1,0},{2,3},{3,2},{4,5},{5,4},{6,7},{7,6},{8,9},{9,8},{10,11... | collective-permute-start | bytes 884744 | tf_op jit(solution)/shard_map/ppermute | solution.py:23
  32.9 27.5 %copy-start.3 = (bf16[2,128,2048]{2,1,0:T(8,128)(2,1)S(1)}, bf16[2,128,2048]{2,1,0:T(8,128)(2,1)}, u32[]{:S(2)}) copy-start(bf16[2,128,2048]{2,1,0:T(8,128)(2,1)} %param.18) | copy-start | bytes 3145732
  32.9 27.5 %copy-start.4 = (bf16[192,2,128]{2,1,0:T(2,128)(2,1)S(1)}, bf16[192,2,128]{2,1,0:T(2,128)(2,1)}, u32[]{:S(2)}) copy-start(bf16[192,2,128]{2,1,0:T(2,128)(2,1)} %refs_1_.2) | copy-start | bytes 294916
  32.9 27.5 %copy-start.5 = (f32[2]{0:T(128)S(1)}, f32[2]{0:T(128)}, u32[]{:S(2)}) copy-start(f32[2]{0:T(128)} %refs_5_.1) | copy-start | bytes 28
  32.9 27.5 %copy-start.6 = (f32[128]{0:T(128)S(1)}, f32[128]{0:T(128)}, u32[]{:S(2)}) copy-start(f32[128]{0:T(128)} %param.17) | copy-start | bytes 1540
  55.1 9.8 %collective-permute-start.24 = (bf16[72,2048]{1,0:T(8,128)(2,1)S(1)}, bf16[72,2048]{1,0:T(8,128)(2,1)S(1)}, u32[]{:S(2)}, u32[]{:S(2)}) collective-permute-start(bf16[72,2048]{1,0:T(8,128)(2,1)S(1)} %shard_map.150.refs_0_), channel_id=1, source_target_pairs={{0,2},{1,3},{2,0},{3,1},{4,6},{5,7},{6,4},{7,5},{8,10},{9,11},{10,... | collective-permute-start | bytes 884744 | tf_op jit(solution)/shard_map/ppermute | solution.py:23
  59.3 11.3 %collective-permute-start.23 = (bf16[72,2048]{1,0:T(8,128)(2,1)S(1)}, bf16[72,2048]{1,0:T(8,128)(2,1)S(1)}, u32[]{:S(2)}, u32[]{:S(2)}) collective-permute-start(bf16[72,2048]{1,0:T(8,128)(2,1)S(1)} %shard_map.150.refs_0_), channel_id=1, source_target_pairs={{0,1},{1,0},{2,3},{3,2},{4,5},{5,4},{6,7},{7,6},{8,9},{9,8},{10,11... | collective-permute-start | bytes 884744 | tf_op jit(solution)/shard_map/ppermute | solution.py:23
  59.8 10.9 %collective-permute-start.16 = (bf16[72,2048]{1,0:T(8,128)(2,1)S(1)}, bf16[72,2048]{1,0:T(8,128)(2,1)S(1)}, u32[]{:S(2)}, u32[]{:S(2)}) collective-permute-start(bf16[72,2048]{1,0:T(8,128)(2,1)S(1)} %shard_map.147.refs_0_), channel_id=1, source_target_pairs={{0,2},{1,3},{2,0},{3,1},{4,6},{5,7},{6,4},{7,5},{8,10},{9,11},{10,... | collective-permute-start | bytes 884744 | tf_op jit(solution)/shard_map/ppermute | solution.py:23
  60.1 6.0 %collective-permute-start.34 = (bf16[72,2048]{1,0:T(8,128)(2,1)S(1)}, bf16[72,2048]{1,0:T(8,128)(2,1)S(1)}, u32[]{:S(2)}, u32[]{:S(2)}) collective-permute-start(bf16[72,2048]{1,0:T(8,128)(2,1)S(1)} %collective-permute-done.33.refs_2_), channel_id=1, source_target_pairs={{0,1},{1,0},{2,3},{3,2},{4,5},{5,4},{6,7},{7,6},{8,9},{9,8},{10,11... | collective-permute-start | bytes 884744 | tf_op jit(solution)/shard_map/ppermute | solution.py:23
  60.4 6.3 %copy-start = (bf16[1,2048,896]{2,1,0:T(8,128)(2,1)S(1)}, bf16[1,2048,896]{2,1,0:T(8,128)(2,1)}, u32[]{:S(2)}) copy-start(bf16[1,2048,896]{2,1,0:T(8,128)(2,1)} %param.23) | copy-start | bytes 11010052
  60.5 6.3 %copy-start.1 = (bf16[1,2048,896]{2,1,0:T(8,128)(2,1)S(1)}, bf16[1,2048,896]{2,1,0:T(8,128)(2,1)}, u32[]{:S(2)}) copy-start(bf16[1,2048,896]{2,1,0:T(8,128)(2,1)} %param.24) | copy-start | bytes 11010052
  60.5 6.3 %copy-start.2 = (bf16[1,896,2048]{2,1,0:T(8,128)(2,1)S(1)}, bf16[1,896,2048]{2,1,0:T(8,128)(2,1)}, u32[]{:S(2)}) copy-start(bf16[1,896,2048]{2,1,0:T(8,128)(2,1)} %param.25) | copy-start | bytes 11010052
  64.7 16.4 %collective-permute-start.15 = (bf16[72,2048]{1,0:T(8,128)(2,1)S(1)}, bf16[72,2048]{1,0:T(8,128)(2,1)S(1)}, u32[]{:S(2)}, u32[]{:S(2)}) collective-permute-start(bf16[72,2048]{1,0:T(8,128)(2,1)S(1)} %shard_map.147.refs_0_), channel_id=1, source_target_pairs={{0,1},{1,0},{2,3},{3,2},{4,5},{5,4},{6,7},{7,6},{8,9},{9,8},{10,11... | collective-permute-start | bytes 884744 | tf_op jit(solution)/shard_map/ppermute | solution.py:23
  65.0 10.8 %collective-permute-start.8 = (bf16[72,2048]{1,0:T(8,128)(2,1)S(1)}, bf16[72,2048]{1,0:T(8,128)(2,1)S(1)}, u32[]{:S(2)}, u32[]{:S(2)}) collective-permute-start(bf16[72,2048]{1,0:T(8,128)(2,1)S(1)} %shard_map.144.refs_0_), channel_id=1, source_target_pairs={{0,2},{1,3},{2,0},{3,1},{4,6},{5,7},{6,4},{7,5},{8,10},{9,11},{10,... | collective-permute-start | bytes 884744 | tf_op jit(solution)/shard_map/ppermute | solution.py:23
  66.2 11.0 %collective-permute-start.25 = (bf16[72,2048]{1,0:T(8,128)(2,1)S(1)}, bf16[72,2048]{1,0:T(8,128)(2,1)S(1)}, u32[]{:S(2)}, u32[]{:S(2)}) collective-permute-start(bf16[72,2048]{1,0:T(8,128)(2,1)S(1)} %collective-permute-done.24.refs_2_), channel_id=1, source_target_pairs={{0,1},{1,0},{2,3},{3,2},{4,5},{5,4},{6,7},{7,6},{8,9},{9,8},{10,11... | collective-permute-start | bytes 884744 | tf_op jit(solution)/shard_map/ppermute | solution.py:23
  70.6 15.2 %collective-permute-start.7 = (bf16[72,2048]{1,0:T(8,128)(2,1)S(1)}, bf16[72,2048]{1,0:T(8,128)(2,1)S(1)}, u32[]{:S(2)}, u32[]{:S(2)}) collective-permute-start(bf16[72,2048]{1,0:T(8,128)(2,1)S(1)} %shard_map.144.refs_0_), channel_id=1, source_target_pairs={{0,1},{1,0},{2,3},{3,2},{4,5},{5,4},{6,7},{7,6},{8,9},{9,8},{10,11... | collective-permute-start | bytes 884744 | tf_op jit(solution)/shard_map/ppermute | solution.py:23
  70.7 10.9 %collective-permute-start.17 = (bf16[72,2048]{1,0:T(8,128)(2,1)S(1)}, bf16[72,2048]{1,0:T(8,128)(2,1)S(1)}, u32[]{:S(2)}, u32[]{:S(2)}) collective-permute-start(bf16[72,2048]{1,0:T(8,128)(2,1)S(1)} %collective-permute-done.16.refs_2_), channel_id=1, source_target_pairs={{0,1},{1,0},{2,3},{3,2},{4,5},{5,4},{6,7},{7,6},{8,9},{9,8},{10,11... | collective-permute-start | bytes 884744 | tf_op jit(solution)/shard_map/ppermute | solution.py:23
  75.8 10.5 %collective-permute-start.9 = (bf16[72,2048]{1,0:T(8,128)(2,1)S(1)}, bf16[72,2048]{1,0:T(8,128)(2,1)S(1)}, u32[]{:S(2)}, u32[]{:S(2)}) collective-permute-start(bf16[72,2048]{1,0:T(8,128)(2,1)S(1)} %collective-permute-done.8.refs_2_), channel_id=1, source_target_pairs={{0,1},{1,0},{2,3},{3,2},{4,5},{5,4},{6,7},{7,6},{8,9},{9,8},{10,11... | collective-permute-start | bytes 884744 | tf_op jit(solution)/shard_map/ppermute | solution.py:23
  77.2 16.5 %collective-permute-start.3 = (bf16[2,48,2048]{2,1,0:T(8,128)(2,1)S(1)}, bf16[2,48,2048]{2,1,0:T(8,128)(2,1)S(1)}, u32[]{:S(2)}, u32[]{:S(2)}) collective-permute-start(bf16[2,48,2048]{2,1,0:T(8,128)(2,1)S(1)} %get-tuple-element.30), channel_id=1, source_target_pairs={{0,1},{1,0},{2,3},{3,2},{4,5},{5,4},{6,7},{7,6},{8,9},{9,8},{10,11... | collective-permute-start | bytes 1179656 | tf_op jit(solution)/shard_map/ppermute | solution.py:23
  81.1 9.2 %collective-permute-start.35 = (bf16[2,72,2048]{2,1,0:T(8,128)(2,1)S(1)}, bf16[2,72,2048]{2,1,0:T(8,128)(2,1)S(1)}, u32[]{:S(2)}, u32[]{:S(2)}) collective-permute-start(bf16[2,72,2048]{2,1,0:T(8,128)(2,1)S(1)} %get-tuple-element.53), channel_id=1, source_target_pairs={{0,1},{1,0},{2,3},{3,2},{4,5},{5,4},{6,7},{7,6},{8,9},{9,8},{10,11... | collective-permute-start | bytes 1769480 | tf_op jit(solution)/shard_map/ppermute | solution.py:23
  81.6 9.0 %collective-permute-start.26 = (bf16[2,72,2048]{2,1,0:T(8,128)(2,1)S(1)}, bf16[2,72,2048]{2,1,0:T(8,128)(2,1)S(1)}, u32[]{:S(2)}, u32[]{:S(2)}) collective-permute-start(bf16[2,72,2048]{2,1,0:T(8,128)(2,1)S(1)} %get-tuple-element.47), channel_id=1, source_target_pairs={{0,1},{1,0},{2,3},{3,2},{4,5},{5,4},{6,7},{7,6},{8,9},{9,8},{10,11... | collective-permute-start | bytes 1769480 | tf_op jit(solution)/shard_map/ppermute | solution.py:23
  85.8 6.2 %collective-permute-start.18 = (bf16[2,72,2048]{2,1,0:T(8,128)(2,1)S(1)}, bf16[2,72,2048]{2,1,0:T(8,128)(2,1)S(1)}, u32[]{:S(2)}, u32[]{:S(2)}) collective-permute-start(bf16[2,72,2048]{2,1,0:T(8,128)(2,1)S(1)} %get-tuple-element.41), channel_id=1, source_target_pairs={{0,1},{1,0},{2,3},{3,2},{4,5},{5,4},{6,7},{7,6},{8,9},{9,8},{10,11... | collective-permute-start | bytes 1769480 | tf_op jit(solution)/shard_map/ppermute | solution.py:23
  90.1 2.3 %collective-permute-start.10 = (bf16[2,72,2048]{2,1,0:T(8,128)(2,1)S(1)}, bf16[2,72,2048]{2,1,0:T(8,128)(2,1)S(1)}, u32[]{:S(2)}, u32[]{:S(2)}) collective-permute-start(bf16[2,72,2048]{2,1,0:T(8,128)(2,1)S(1)} %get-tuple-element.35), channel_id=1, source_target_pairs={{0,1},{1,0},{2,3},{3,2},{4,5},{5,4},{6,7},{7,6},{8,9},{9,8},{10,11... | collective-permute-start | bytes 1769480 | tf_op jit(solution)/shard_map/ppermute | solution.py:23
  90.3 8.2 %collective-permute-start.36 = (bf16[72,2048]{1,0:T(8,128)(2,1)S(1)}, bf16[72,2048]{1,0:T(8,128)(2,1)S(1)}, u32[]{:S(2)}, u32[]{:S(2)}) collective-permute-start(bf16[72,2048]{1,0:T(8,128)(2,1)S(1)} %fusion.4), channel_id=1, source_target_pairs={{0,2},{1,3},{2,0},{3,1},{4,6},{5,7},{6,4},{7,5},{8,10},{9,11},{10,... | collective-permute-start | bytes 884744 | tf_op jit(solution)/shard_map/ppermute | solution.py:23
  90.7 14.1 %collective-permute-start.27 = (bf16[72,2048]{1,0:T(8,128)(2,1)S(1)}, bf16[72,2048]{1,0:T(8,128)(2,1)S(1)}, u32[]{:S(2)}, u32[]{:S(2)}) collective-permute-start(bf16[72,2048]{1,0:T(8,128)(2,1)S(1)} %fusion.3), channel_id=1, source_target_pairs={{0,2},{1,3},{2,0},{3,1},{4,6},{5,7},{6,4},{7,5},{8,10},{9,11},{10,... | collective-permute-start | bytes 884744 | tf_op jit(solution)/shard_map/ppermute | solution.py:23
  92.1 19.1 %collective-permute-start.19 = (bf16[72,2048]{1,0:T(8,128)(2,1)S(1)}, bf16[72,2048]{1,0:T(8,128)(2,1)S(1)}, u32[]{:S(2)}, u32[]{:S(2)}) collective-permute-start(bf16[72,2048]{1,0:T(8,128)(2,1)S(1)} %fusion.2), channel_id=1, source_target_pairs={{0,2},{1,3},{2,0},{3,1},{4,6},{5,7},{6,4},{7,5},{8,10},{9,11},{10,... | collective-permute-start | bytes 884744 | tf_op jit(solution)/shard_map/ppermute | solution.py:23
  92.5 25.0 %collective-permute-start.11 = (bf16[72,2048]{1,0:T(8,128)(2,1)S(1)}, bf16[72,2048]{1,0:T(8,128)(2,1)S(1)}, u32[]{:S(2)}, u32[]{:S(2)}) collective-permute-start(bf16[72,2048]{1,0:T(8,128)(2,1)S(1)} %fusion.1), channel_id=1, source_target_pairs={{0,2},{1,3},{2,0},{3,1},{4,6},{5,7},{6,4},{7,5},{8,10},{9,11},{10,... | collective-permute-start | bytes 884744 | tf_op jit(solution)/shard_map/ppermute | solution.py:23
  93.8 27.9 %collective-permute-start.4 = (bf16[48,2048]{1,0:T(8,128)(2,1)S(1)}, bf16[48,2048]{1,0:T(8,128)(2,1)S(1)}, u32[]{:S(2)}, u32[]{:S(2)}) collective-permute-start(bf16[48,2048]{1,0:T(8,128)(2,1)S(1)} %fusion.5), channel_id=1, source_target_pairs={{0,2},{1,3},{2,0},{3,1},{4,6},{5,7},{6,4},{7,5},{8,10},{9,11},{10,... | collective-permute-start | bytes 589832 | tf_op jit(solution)/shard_map/ppermute | solution.py:23
  98.7 24.3 %collective-permute-start.37 = (bf16[72,1024]{1,0:T(8,128)(2,1)S(1)}, bf16[72,1024]{1,0:T(8,128)(2,1)S(1)}, u32[]{:S(2)}, u32[]{:S(2)}) collective-permute-start(bf16[72,1024]{1,0:T(8,128)(2,1)S(1)} %get-tuple-element.54), channel_id=1, source_target_pairs={{0,16},{4,20},{8,24},{12,28},{16,0},{20,4},{24,8},{28,12},{1,17},{... | collective-permute-start | bytes 442376 | tf_op jit(solution)/shard_map/ppermute | solution.py:23
  104.8 18.1 %collective-permute-start.38 = (bf16[72,1024]{1,0:T(8,128)(2,1)S(1)}, bf16[72,1024]{1,0:T(8,128)(2,1)S(1)}, u32[]{:S(2)}, u32[]{:S(2)}) collective-permute-start(bf16[72,1024]{1,0:T(8,128)(2,1)S(1)} %get-tuple-element.55), channel_id=1, source_target_pairs={{0,20},{4,16},{8,28},{12,24},{16,4},{20,0},{24,12},{28,8},{1,21},{... | collective-permute-start | bytes 442376 | tf_op jit(solution)/shard_map/ppermute | solution.py:23
  111.2 13.9 %collective-permute-start.28 = (bf16[72,1024]{1,0:T(8,128)(2,1)S(1)}, bf16[72,1024]{1,0:T(8,128)(2,1)S(1)}, u32[]{:S(2)}, u32[]{:S(2)}) collective-permute-start(bf16[72,1024]{1,0:T(8,128)(2,1)S(1)} %get-tuple-element.48), channel_id=1, source_target_pairs={{0,8},{4,12},{8,0},{12,4},{16,24},{20,28},{24,16},{28,20},{1,9},{5... | collective-permute-start | bytes 442376 | tf_op jit(solution)/shard_map/ppermute | solution.py:23
  117.5 7.6 %collective-permute-start.29 = (bf16[72,1024]{1,0:T(8,128)(2,1)S(1)}, bf16[72,1024]{1,0:T(8,128)(2,1)S(1)}, u32[]{:S(2)}, u32[]{:S(2)}) collective-permute-start(bf16[72,1024]{1,0:T(8,128)(2,1)S(1)} %get-tuple-element.49), channel_id=1, source_target_pairs={{0,12},{4,8},{8,4},{12,0},{16,28},{20,24},{24,20},{28,16},{1,13},{... | collective-permute-start | bytes 442376 | tf_op jit(solution)/shard_map/ppermute | solution.py:23
  121.7 6.6 %collective-permute-start.20 = (bf16[72,1024]{1,0:T(8,128)(2,1)S(1)}, bf16[72,1024]{1,0:T(8,128)(2,1)S(1)}, u32[]{:S(2)}, u32[]{:S(2)}) collective-permute-start(bf16[72,1024]{1,0:T(8,128)(2,1)S(1)} %get-tuple-element.43), channel_id=1, source_target_pairs={{0,4},{4,0},{8,12},{12,8},{16,20},{20,16},{24,28},{28,24},{1,5},{5... | collective-permute-start | bytes 442376 | tf_op jit(solution)/shard_map/ppermute | solution.py:23
  123.0 10.8 %collective-permute-start.12 = (bf16[72,1024]{1,0:T(8,128)(2,1)S(1)}, bf16[72,1024]{1,0:T(8,128)(2,1)S(1)}, u32[]{:S(2)}, u32[]{:S(2)}) collective-permute-start(bf16[72,1024]{1,0:T(8,128)(2,1)S(1)} %get-tuple-element.36), channel_id=1, source_target_pairs={{0,24},{4,28},{8,16},{12,20},{16,8},{20,12},{24,0},{28,4},{1,25},{... | collective-permute-start | bytes 442376 | tf_op jit(solution)/shard_map/ppermute | solution.py:23
  123.0 14.2 %collective-permute-start.13 = (bf16[72,1024]{1,0:T(8,128)(2,1)S(1)}, bf16[72,1024]{1,0:T(8,128)(2,1)S(1)}, u32[]{:S(2)}, u32[]{:S(2)}) collective-permute-start(bf16[72,1024]{1,0:T(8,128)(2,1)S(1)} %get-tuple-element.37), channel_id=1, source_target_pairs={{0,28},{4,24},{8,20},{12,16},{16,12},{20,8},{24,4},{28,0},{1,29},{... | collective-permute-start | bytes 442376 | tf_op jit(solution)/shard_map/ppermute | solution.py:23
